TPU v7x, 32 devices: a whole 2x2x4 slice. The times are simulated.
32 devices in a mesh: sp: 4 (over y, x), tp: 8 (over z, core).
Axes of the slice: x: 2, y: 2, z: 4, core: 2. Of those that a mesh axis runs over, the one named last changes fastest.
Arguments:
- tokens: bfloat16 [8, 512, 4096], P('tp', 'sp'), may hold values from -6 to 6
- latent_down_matrix: bfloat16 [4096, 512], P('tp'), may hold values from -0.09375 to 0.09375
- rope_weight: bfloat16 [4096, 64], P('tp'), may hold values from -0.09375 to 0.09375
- latent_norm_scale: float32 [512], replicated, may hold values from 0.1 to 1.9
- key_up_matrix: bfloat16 [512, 32, 128], P(None, 'tp'), may hold values from -0.25 to 0.25
- value_up_matrix: bfloat16 [512, 32, 128], P(None, 'tp'), may hold values from -0.25 to 0.25
- query: bfloat16 [8, 32, 192], P('sp', 'tp'), may hold values from -126 to 126
Outputs:
- plain_key_cache: bfloat16 [8, 512, 32, 128], P('sp', None, 'tp')
- head_value_cache: bfloat16 [8, 512, 32, 128], P('sp', None, 'tp')
- rotated_key_cache: bfloat16 [8, 512, 64], P('sp')
- first_read: bfloat16 [8, 32, 128], P('sp', 'tp')
All inputs are finite; a program needn't handle non-finite values.
Results may differ from a plain program's by a relative error of at most 0.035.
Values may be sent and summed in bfloat16 or wider, within the bound.
A program may use at most 64 MiB of HBM per device.

v0:
```python
import functools

import numpy as np
import jax
import jax.numpy as jnp
from jax import lax
from jax.sharding import PartitionSpec as P
from jax.experimental import pallas as pl
from jax.experimental.pallas import tpu as pltpu

CORES = 2
PARTS = 4
BF16 = jnp.bfloat16
F32 = jnp.float32


def turn_tables(positions, width):
    half = width // 2
    freqs = (1.0 / np.float32(10000.0) ** (np.arange(half, dtype=np.float32) * np.float32(2.0) / np.float32(width))).astype(np.float32)
    angles = positions.astype(np.float32)[:, None] * freqs
    cosine = np.cos(angles).astype(np.float32)
    sine = np.sin(angles).astype(np.float32)
    return np.concatenate([cosine, cosine], -1), np.concatenate([-sine, sine], -1)


def turn(part, cosine, sine):
    half = part.shape[-1] // 2
    swapped = jnp.concatenate([part[:, half:], part[:, :half]], axis=-1)
    return part * cosine + swapped * sine


def move_kernel(planes, spots, tok, wl, wr, scale, cos_hbm, sin_hbm, kup, vup, x_out, rot_out, up_out,
                tokens, wlat, wrope, acc, acct, other, othert, spread, spreadt, kbuf, vbuf, upbuf, cos_ref, sin_ref,
                tok_s, tok_r, own_s, z_s, z_r, zo_s, x_s, x_r, y_s, y_r, dx_s, dx_r, dy_s, dy_r,
                acc_s, acc_r, g_s, g_r, f_s, f_r, p_s, p_r, up_s):
    s = lax.axis_index("sp")
    t = lax.axis_index("tp")
    z = t // CORES
    c = t % CORES
    rows, lat = wl.shape
    rope = wr.shape[0]
    span = tok.shape[1]
    quarter = rows // 4
    eighth = quarter // 2
    rpart = rope // 4
    half = span // PARTS
    q = s % 4
    sx = s + 1 - 2 * (s % 2)
    sy = s + 2 - 4 * ((s // 2) % 2)
    qx = q + 1 - 2 * (q % 2)
    qy = q + 2 - 4 * (q // 2)
    qd = 3 - q

    def dev(si, zi, ci):
        return {"sp": si, "tp": zi * CORES + ci}

    here = dev(s, z, 1 - c)

    def remote(src, dst, ss, rs, where):
        return pltpu.make_async_remote_copy(
            src_ref=src, dst_ref=dst, send_sem=ss, recv_sem=rs,
            device_id=where, device_id_type=pl.DeviceIdType.MESH)

    def own_tok(u):
        cols = pl.ds(pl.multiple_of((u * CORES + c) * rows, 128), rows)
        return pltpu.make_async_copy(tok.at[0, :, cols], tokens.at[0, u], own_s.at[u])

    def part_tok(u):
        cols = pl.ds(pl.multiple_of((u * CORES + 1 - c) * rows, 128), rows)
        return remote(tok.at[0, :, cols], tokens.at[1, u], tok_s.at[u], tok_r.at[u], here)

    own_wl = pltpu.make_async_copy(wl, wlat.at[z], own_s.at[planes])
    own_wr = pltpu.make_async_copy(wr, wrope.at[z], own_s.at[planes + 1])
    place = pl.ds(pl.multiple_of(s * span, 128), span)
    get_k = pltpu.make_async_copy(kup, kbuf, up_s.at[0])
    get_v = pltpu.make_async_copy(vup, vbuf, up_s.at[1])
    get_c = pltpu.make_async_copy(cos_hbm.at[:, place], cos_ref, up_s.at[2])
    get_n = pltpu.make_async_copy(sin_hbm.at[:, place], sin_ref, up_s.at[3])
    own_wl.start()
    own_wr.start()

    barrier = pltpu.get_barrier_semaphore()

    def greet(where):
        pl.semaphore_signal(barrier, inc=1, device_id=where, device_id_type=pl.DeviceIdType.MESH)

    for i in range(1, planes):
        greet(dev(s, lax.rem(z + i, planes), c))
    for i in range(1, spots):
        greet(dev(lax.rem(s + i, spots), z, c))
    greet(here)
    for u in range(planes):
        own_tok(u).start()
    own_wl.wait()
    own_wr.wait()
    pl.semaphore_wait(barrier, planes - 1 + spots - 1 + 1)

    def piece(u, part, k, ss, rs, where):
        rng = pl.ds(pl.multiple_of(part * quarter + k * eighth, 16), eighth)
        out = [remote(wlat.at[u, rng], wlat.at[u, rng], ss.at[k, u], rs.at[k, u], where)]
        if k == 0:
            rng = pl.ds(pl.multiple_of(part * rpart, 16), rpart)
            out.append(remote(wrope.at[u, rng], wrope.at[u, rng], ss.at[2, u], rs.at[2, u], where))
        return out

    def each(copies, what):
        for p in copies:
            getattr(p, what)()

    def z_rows(k):
        start = q * quarter + k * eighth if k < 2 else qd * quarter + eighth
        return pl.ds(pl.multiple_of(start, 16), eighth)

    def z_piece(u, k, sems, where):
        rng = z_rows(k)
        i = k if k < 2 else 3
        out = [remote(wlat.at[u, rng], wlat.at[u, rng], sems(i), z_r.at[i, u], where)]
        if k == 0:
            rng = pl.ds(pl.multiple_of(q * rpart, 16), rpart)
            out.append(remote(wrope.at[u, rng], wrope.at[u, rng], sems(2), z_r.at[2, u], where))
        return out

    def z_own(k):
        return z_piece(z, k, lambda i: zo_s.at[i], dev(s, z + 1, c))

    def z_up(u, k):
        return z_piece(u, k, lambda i: z_s.at[i, u], dev(s, z + 1, c))

    def z_down(u, k):
        return z_piece(u, k, lambda i: z_s.at[i, u], dev(s, z - 1, c))

    def z_in(u, k):
        return z_piece(u, k, lambda i: z_s.at[i, u], here)

    def by_y(u):
        return (u + c) % 2 == 0

    def x_copy(u, k):
        return piece(u, q, k, x_s, x_r, dev(sx, z, c))

    def y_copy(u, k):
        return piece(u, q, k, y_s, y_r, dev(sy, z, c))

    def x_in(u, k):
        return piece(u, qx, k, x_s, x_r, here)

    def y_in(u, k):
        return piece(u, qy, k, y_s, y_r, here)

    def dy_copy(u):
        return piece(u, qx, 0, dy_s, dy_r, dev(sy, z, c))

    def dx_copy(u):
        return piece(u, qy, 0, dx_s, dx_r, dev(sx, z, c))

    def dy_in(u):
        return piece(u, qd, 0, dy_s, dy_r, here)

    def dx_in(u):
        return piece(u, qd, 0, dx_s, dx_r, here)

    has_up = z + 1 < planes
    has_down = z > 0
    for k in range(2):
        @pl.when(has_up)
        def _():
            each(z_own(k), "start")

        @pl.when(has_down)
        def _():
            each(z_down(z, k), "start")

    for u in range(planes):
        part_tok(u).start()
    get_k.start()
    get_v.start()
    get_c.start()
    get_n.start()
    contract = (((1,), (1,)), ((), ()))

    def block_dot(u):
        x = tokens[:, u].reshape(CORES * span, rows)
        return (jnp.dot(x, wlat[u], preferred_element_type=F32),
                lax.dot_general(wrope[u], x, contract, preferred_element_type=F32))

    def own_block():
        for u in range(planes):
            own_tok(u).wait()
            part_tok(u).wait()
        a, b = block_dot(z)
        acc[...] = a
        acct[...] = b

    put_up = pltpu.make_async_copy(upbuf, up_out, up_s.at[4])

    def reshape_up():
        get_k.wait()
        get_v.wait()
        get_c.wait()
        get_n.wait()
        heads, kw = kbuf.shape[1:]
        vw = vbuf.shape[2]
        k = kbuf[...].astype(F32)
        v = vbuf[...].astype(F32)
        for h in range(heads):
            upbuf[:, h * kw:(h + 1) * kw] = k[:, h, :].astype(BF16)
            upbuf[:, heads * kw + h * vw:heads * kw + (h + 1) * vw] = v[:, h, :].astype(BF16)
        put_up.start()

    def relay(u, k, sign):
        each(z_in(u, k), "wait_recv")
        if sign < 0:
            @pl.when(has_up)
            def _():
                each(z_up(u, k), "start")
        else:
            @pl.when(has_down)
            def _():
                each(z_down(u, k), "start")

    def send_own(k):
        @pl.when(has_up)
        def _():
            each(z_own(k), "start")

        @pl.when(has_down)
        def _():
            each(z_down(z, k), "start")

    def valid(u):
        return (u >= 0) & (u < planes)

    def step(d, carry):
        for k in range(2):
            for sign in (-1, 1):
                u = z + sign * d

                @pl.when(valid(u))
                def _():
                    relay(u, k, sign)
                    each(x_copy(u, k), "start")
                    each(y_copy(u, k), "start")

        @pl.when(d == 1)
        def _():
            own_block()

        @pl.when(d == 2)
        def _():
            reshape_up()

        @pl.when(d == planes - 1)
        def _():
            send_own(2)

        for sign in (-1, 1):
            u = z + sign * (d - 1)

            @pl.when(valid(u) & (d > 1))
            def _():
                @pl.when(by_y(u))
                def _():
                    each(x_in(u, 0), "wait_recv")
                    each(dy_copy(u), "start")

                @pl.when(~by_y(u))
                def _():
                    each(y_in(u, 0), "wait_recv")
                    each(dx_copy(u), "start")
        return carry

    lax.fori_loop(1, planes + 1, step, 0)

    def finish(d, carry):
        for sign in (-1, 1):
            u = z + sign * d

            @pl.when(valid(u))
            def _():
                relay(u, 2, sign)
        for sign in (-1, 1):
            u = z + sign * d

            @pl.when(valid(u))
            def _():
                each(x_in(u, 1), "wait_recv")
                each(y_in(u, 1), "wait_recv")

                @pl.when(by_y(u))
                def _():
                    each(y_in(u, 0), "wait_recv")
                    each(dy_in(u), "wait_recv")

                @pl.when(~by_y(u))
                def _():
                    each(x_in(u, 0), "wait_recv")
                    each(dx_in(u), "wait_recv")
                a, b = block_dot(u)
                acc[...] += a
                acct[...] += b
        return carry

    lax.fori_loop(1, planes, finish, 0)

    swaps = [remote(acc.at[pl.ds(span, span)], other, acc_s.at[0], acc_r.at[0], here),
             remote(acct.at[:, pl.ds(span, span)], othert, acc_s.at[1], acc_r.at[1], here)]
    each(swaps, "start")
    each(swaps, "wait")
    latent = acc[:span] + other[...]
    ropes = acct[:, :span] + othert[...]
    scaled = latent * lax.rsqrt(jnp.mean(latent * latent, axis=-1, keepdims=True) + 1e-06)
    spread[z] = (scaled * scale[...]).astype(BF16)
    swapped = jnp.concatenate([ropes[rope // 2:], ropes[:rope // 2]], axis=0)
    spreadt[z] = (ropes * cos_ref[...] + swapped * sin_ref[...]).astype(BF16)

    def g_copy(u, k, zi, slot):
        rng = pl.ds(k * half, half)
        out = [remote(spread.at[u, rng], spread.at[u, rng], g_s.at[slot, k, u], g_r.at[k, u], dev(s, zi, c))]
        if k == 0:
            out.append(remote(spreadt.at[u], spreadt.at[u], g_s.at[slot, PARTS, u], g_r.at[PARTS, u], dev(s, zi, c)))
        return out

    def lanes(si):
        return pl.ds(pl.multiple_of(si * span, 128), span)

    def f_copy(u, k, where, si):
        rng = pl.ds(k * half, half)
        out = [remote(spread.at[u, rng], x_out.at[c, si, rng], f_s.at[k, u], f_r.at[k, si], where)]
        if k == 0:
            out.append(remote(spreadt.at[u], rot_out.at[c, :, lanes(si)], f_s.at[PARTS, u], f_r.at[PARTS, si], where))
        return out

    def p_copy(ci, si, k):
        rng = pl.ds(k * half, half)
        out = [remote(x_out.at[ci, si, rng], x_out.at[ci, si, rng], p_s.at[k, si], p_r.at[k, si], here)]
        if k == 0:
            part = rot_out.at[ci, :, lanes(si)]
            out.append(remote(part, part, p_s.at[PARTS, si], p_r.at[PARTS, si], here))
        return out

    own_copies = [pltpu.make_async_copy(spread.at[s], x_out.at[c, s], own_s.at[0]),
                  pltpu.make_async_copy(spreadt.at[s], rot_out.at[c, :, lanes(s)], own_s.at[1])]

    def deliver(u, k):
        @pl.when(u != s)
        def _():
            each(f_copy(u, k, dev(u, z, c), s), "start")

        if k == PARTS - 1:
            @pl.when(u == s)
            def _():
                each(own_copies, "start")

    for k in range(PARTS):
        @pl.when(has_up)
        def _():
            each(g_copy(z, k, z + 1, 0), "start")

        @pl.when(has_down)
        def _():
            each(g_copy(z, k, z - 1, 1), "start")

        deliver(z, k)

    def g_step(d, carry):
        for k in range(PARTS):
            for sign in (-1, 1):
                u = z + sign * d

                @pl.when((u >= 0) & (u < planes))
                def _():
                    each(g_copy(u, k, z, 0), "wait_recv")
                    if sign < 0:
                        @pl.when(has_up)
                        def _():
                            each(g_copy(u, k, z + 1, 0), "start")
                    else:
                        @pl.when(has_down)
                        def _():
                            each(g_copy(u, k, z - 1, 1), "start")
                    deliver(u, k)
        return carry

    lax.fori_loop(1, planes, g_step, 0)
    each(own_copies, "wait")
    for k in range(PARTS):
        each(p_copy(c, s, k), "start")

    for k in range(PARTS):
        def p_step(i, carry):
            si = lax.rem(s + i, spots)
            each(f_copy(0, k, here, si), "wait_recv")
            each(p_copy(c, si, k), "start")
            return carry

        lax.fori_loop(1, spots, p_step, 0)

    def p_drain(si, carry):
        for k in range(PARTS):
            each(p_copy(1 - c, si, k), "wait_recv")
            each(p_copy(c, si, k), "wait_send")
        return carry

    lax.fori_loop(0, spots, p_drain, 0)

    def drain(u, carry):
        for k in range(PARTS):
            @pl.when(u != s)
            def _():
                each(f_copy(u, k, here, s), "wait_send")

            @pl.when((u <= z) & has_up)
            def _():
                each(g_copy(u, k, z, 0), "wait_send")

            @pl.when((u >= z) & has_down)
            def _():
                each(g_copy(u, k, z, 1), "wait_send")

        for k in range(3):
            @pl.when((u >= z) & has_down)
            def _():
                each(z_down(u, k), "wait_send")

            @pl.when((u < z) & has_up)
            def _():
                each(z_up(u, k), "wait_send")

        for k in range(2):
            @pl.when(u != z)
            def _():
                each(x_copy(u, k), "wait_send")
                each(y_copy(u, k), "wait_send")

        @pl.when((u != z) & by_y(u))
        def _():
            each(dy_copy(u), "wait_send")

        @pl.when((u != z) & ~by_y(u))
        def _():
            each(dx_copy(u), "wait_send")
        return carry

    lax.fori_loop(0, planes, drain, 0)
    put_up.wait()

    @pl.when(has_up)
    def _():
        for k in range(3):
            each(z_own(k), "wait_send")


def read_kernel(x_ref, r_ref, up_ref, q_ref, cos_ref, sin_ref, plain_ref, value_ref, rot_ref, read_ref, wide):
    length = x_ref.shape[1]
    heads = q_ref.shape[1]
    lat = up_ref.shape[0]
    rope = r_ref.shape[1]
    kw = q_ref.shape[2] - rope
    vw = up_ref.shape[1] // heads - kw
    rotated = r_ref[0]
    rot_ref[0] = rotated
    normed = x_ref[0]
    keys = jnp.dot(normed, up_ref[:, :heads * kw], preferred_element_type=F32)
    values = jnp.dot(normed, up_ref[:, heads * kw:], preferred_element_type=F32)
    for h in range(heads):
        wide[pl.ds(h, length, stride=heads), :] = keys[:, h * kw:(h + 1) * kw]
    plain_ref[0] = wide[...].astype(BF16)
    for h in range(heads):
        wide[pl.ds(h, length, stride=heads), :] = values[:, h * vw:(h + 1) * vw]
    value_ref[0] = wide[...].astype(BF16)
    keys = keys.astype(BF16)
    values = values.astype(BF16)
    query = q_ref[0].astype(F32)
    turned = turn(query[:, kw:], cos_ref[...], sin_ref[...]).astype(BF16)
    tiled = jnp.concatenate([query[:, :kw]] * heads, axis=1)
    row = lax.broadcasted_iota(jnp.int32, tiled.shape, 0)
    col = lax.broadcasted_iota(jnp.int32, tiled.shape, 1)
    blocked = jnp.where(col // kw == row, tiled, 0.0).astype(BF16)
    contract = (((1,), (1,)), ((), ()))
    scores = lax.dot_general(blocked, keys, contract, preferred_element_type=F32)
    scores = scores + jnp.dot(turned, rotated, preferred_element_type=F32)
    scores = scores * (1.0 / (kw + rope) ** 0.5)
    weights = jnp.exp(scores - jnp.max(scores, axis=-1, keepdims=True))
    total = jnp.sum(weights, axis=-1, keepdims=True)
    mixed = jnp.dot(weights.astype(BF16), values, preferred_element_type=F32) / total
    for h in range(heads):
        read_ref[0, h:h + 1, :] = mixed[h:h + 1, h * vw:(h + 1) * vw].astype(BF16)


def body(planes, spots, tokens, latent_down, rope_weight, norm_scale, key_up, value_up, query):
    span = tokens.shape[1]
    rows, lat = latent_down.shape
    rope = rope_weight.shape[1]
    heads, kw = key_up.shape[1:]
    vw = value_up.shape[2]
    length = spots * span
    cosine, sine = turn_tables(np.arange(length + 1), rope)
    vmem = pl.BlockSpec(memory_space=pltpu.VMEM)
    hbm = pl.BlockSpec(memory_space=pl.ANY)
    dma = pltpu.SemaphoreType.DMA
    x_all, rot_all, up = pl.pallas_call(
        functools.partial(move_kernel, planes, spots),
        out_shape=(jax.ShapeDtypeStruct((CORES, spots, span, lat), BF16),
                   jax.ShapeDtypeStruct((CORES, rope, length), BF16),
                   jax.ShapeDtypeStruct((lat, heads * (kw + vw)), BF16)),
        in_specs=[hbm, hbm, hbm, vmem, hbm, hbm, hbm, hbm],
        out_specs=(vmem, vmem, hbm),
        scratch_shapes=[
            pltpu.VMEM((CORES, planes, span, rows), BF16),
            pltpu.VMEM((planes, rows, lat), BF16),
            pltpu.VMEM((planes, rope, rows), BF16),
            pltpu.VMEM((CORES * span, lat), F32),
            pltpu.VMEM((rope, CORES * span), F32),
            pltpu.VMEM((span, lat), F32),
            pltpu.VMEM((rope, span), F32),
            pltpu.VMEM((planes, span, lat), BF16),
            pltpu.VMEM((planes, rope, span), BF16),
            pltpu.VMEM(key_up.shape, BF16),
            pltpu.VMEM(value_up.shape, BF16),
            pltpu.VMEM((lat, heads * (kw + vw)), BF16),
            pltpu.VMEM((rope, span), F32),
            pltpu.VMEM((rope, span), F32),
            dma((planes,)), dma((planes,)), dma((planes + 2,)),
            dma((4, planes)), dma((4, planes)), dma((4,)),
            dma((3, planes)), dma((3, planes)), dma((3, planes)), dma((3, planes)),
            dma((3, planes)), dma((3, planes)), dma((3, planes)), dma((3, planes)),
            dma((2,)), dma((2,)),
            dma((2, PARTS + 1, planes)), dma((PARTS + 1, planes)),
            dma((PARTS + 1, planes)), dma((PARTS + 1, spots)),
            dma((PARTS + 1, spots)), dma((PARTS + 1, spots)),
            dma((5,)),
        ],
        compiler_params=pltpu.CompilerParams(collective_id=0, has_side_effects=True),
    )(tokens, latent_down, rope_weight.T, norm_scale.reshape(1, lat),
      jnp.asarray(np.ascontiguousarray(cosine[:length].T)), jnp.asarray(np.ascontiguousarray(sine[:length].T)),
      key_up, value_up)
    x_all = x_all.reshape(CORES, length, lat)

    def whole(shape):
        return pl.BlockSpec(shape, lambda i: (0,) * len(shape))

    def per(shape):
        return pl.BlockSpec((1,) + shape, lambda i: (i,) + (0,) * len(shape))

    plain, value, rot, read = pl.pallas_call(
        read_kernel,
        grid=(CORES,),
        out_shape=(jax.ShapeDtypeStruct((CORES, length * heads, kw), BF16),
                   jax.ShapeDtypeStruct((CORES, length * heads, vw), BF16),
                   jax.ShapeDtypeStruct((CORES, rope, length), BF16),
                   jax.ShapeDtypeStruct((CORES, heads, vw), BF16)),
        in_specs=[per((length, lat)), per((rope, length)), whole(up.shape), per(query.shape[1:]), whole((1, rope)), whole((1, rope))],
        out_specs=(per((length * heads, kw)), per((length * heads, vw)), per((rope, length)), per((heads, vw))),
        scratch_shapes=[pltpu.VMEM((length * heads, kw), F32)],
    )(x_all, rot_all, up, query, jnp.asarray(cosine[length:]), jnp.asarray(sine[length:]))
    return (plain.reshape(CORES, length, heads, kw), value.reshape(CORES, length, heads, vw), jnp.swapaxes(rot, 1, 2), read)


def solution(mesh):
    planes = mesh.shape["tp"] // CORES
    spots = mesh.shape["sp"]
    assert planes == spots and spots % 4 == 0
    in_specs = (
        P("tp", "sp", None),
        P("tp", None),
        P("tp", None),
        P(),
        P(None, "tp", None),
        P(None, "tp", None),
        P("sp", "tp", None),
    )
    out_specs = (
        P("sp", None, "tp", None),
        P("sp", None, "tp", None),
        P("sp", None, None),
        P("sp", "tp", None),
    )
    return jax.shard_map(functools.partial(body, planes, spots), mesh=mesh, in_specs=in_specs,
                         out_specs=out_specs, check_vma=False)
```

profile of v0, /device:TPU:7, one launch (start us, length us, event | category | flops | bytes accessed | tf_op | source)
XLA Modules:
  0.0 54.8 jit_solution(1030915042310033166)
XLA Ops:
  0.6 49.5 %shard_map.138 = (bf16[2,4,128,512]{3,2,1,0:T(8,128)(2,1)}, bf16[2,64,512]{2,1,0:T(8,128)(2,1)}, bf16[512,1024]{1,0:T(8,128)(2,1)}) custom-call(bf16[1,128,4096]{2,1,0:T(8,128)(2,1)} %tok.1, bf16[512,512]{1,0:T(8,128)(2,1)} %wl.1, bf16[64,512]{1,0:T(8,128)(2,1)} %bitcast.7, f32[1,512]{1,0:T(1,128)} %bitcast.8, f32[64,512]{1,0:T(8,128)} %constant.8.clone.cos_hbm, ...), custom_call_target="tpu_custom_call" | custom-call | tf_op jit(solution)/shard_map/pallas_call | solution.py:501
  50.1 4.7 %shard_map.139 = (bf16[2,2048,128]{2,1,0:T(8,128)(2,1)}, bf16[2,2048,128]{2,1,0:T(8,128)(2,1)}, bf16[2,64,512]{2,1,0:T(8,128)(2,1)}, bf16[2,4,128]{2,1,0:T(4,128)(2,1)}) custom-call(bf16[2,512,512]{2,1,0:T(8,128)(2,1)} %bitcast.6, bf16[2,64,512]{2,1,0:T(8,128)(2,1)} %get-tuple-element.12.r_ref, bf16[512,1024]{1,0:T(8,128)(2,1)} %get-tuple-element.13.up_ref, ...), custom_call_target="tpu_custom_call" | custom-call | tf_op jit(solution)/shard_map/pallas_call | solution.py:545
where the time goes:
time: 54.9 us; the launch traced here: 54.8 us
  Pallas kernels  54.1 us (99%)
  between operations  0.64 us (1%)
    pallas_call x1, Pallas kernels, body(): pl.pallas_call(functools.partial(move_kernel, planes, spots), out_shape=(...  49.5 us
    pallas_call x1, Pallas kernels, body(): pl.pallas_call(read_kernel, grid=(CORES,), out_shape=(jax.ShapeDtypeStruc...  4.65 us

commit v1 on v0

v1 whole, which is shorter than its diff:
```python
import functools

import numpy as np
import jax
import jax.numpy as jnp
from jax import lax
from jax.sharding import PartitionSpec as P
from jax.experimental import pallas as pl
from jax.experimental.pallas import tpu as pltpu

CORES = 2
PARTS = 4
LAG = 4
VMEM_BYTES = 32 * 1024 * 1024
BF16 = jnp.bfloat16
F32 = jnp.float32


def turn_tables(positions, width):
    half = width // 2
    freqs = (1.0 / np.float32(10000.0) ** (np.arange(half, dtype=np.float32) * np.float32(2.0) / np.float32(width))).astype(np.float32)
    angles = positions.astype(np.float32)[:, None] * freqs
    cosine = np.cos(angles).astype(np.float32)
    sine = np.sin(angles).astype(np.float32)
    return np.concatenate([cosine, cosine], -1), np.concatenate([-sine, sine], -1)


def turn(part, cosine, sine):
    half = part.shape[-1] // 2
    swapped = jnp.concatenate([part[:, half:], part[:, :half]], axis=-1)
    return part * cosine + swapped * sine


def move_kernel(planes, spots, tok, wl, wr, scale_hbm, cos_hbm, sin_hbm, cosq_hbm, sinq_hbm, kup, vup, q_hbm,
                k_out, v_out, flat_out, score_out, rot_out, turned_out,
                tokens, wlat, wrope, acc, acct, other, othert, spread, spreadt, xall, between, betweent,
                kbuf, vbuf, up, qbuf, blocked, wide, cos_ref, sin_ref, cosq, sinq, scale,
                tok_s, tok_r, own_s, zu_s, zd_s, z_r, x_s, x_r, y_s, y_r, d_s, d_r,
                acc_s, acc_r, g_s, g_r, j_s, f_s, f_r, m_s, m_r, p_s, p_r, up_s):
    s = lax.axis_index("sp")
    t = lax.axis_index("tp")
    z = t // CORES
    c = t % CORES
    near = spots == 4
    rows, lat = wl.shape
    rope = wr.shape[0]
    span = tok.shape[1]
    heads, kw = kup.shape[1:]
    vw = vup.shape[2]
    quarter = rows // 4
    eighth = quarter // 2
    rpart = rope // 4
    part = span // PARTS
    q = s % 4
    sx = s + 1 - 2 * (s % 2)
    sy = s + 2 - 4 * ((s // 2) % 2)
    sd = sx + sy - s
    qx = q + 1 - 2 * (q % 2)
    qy = q + 2 - 4 * (q // 2)
    qd = 3 - q
    has_up = z + 1 < planes
    has_down = z > 0

    def dev(si, zi, ci):
        return {"sp": si, "tp": zi * CORES + ci}

    here = dev(s, z, 1 - c)
    barrier = pltpu.get_barrier_semaphore()

    def greet(where):
        pl.semaphore_signal(barrier, inc=1, device_id=where, device_id_type=pl.DeviceIdType.MESH)

    @pl.when(has_up)
    def _():
        greet(dev(s, z + 1, c))

    @pl.when(has_down)
    def _():
        greet(dev(s, z - 1, c))

    if near:
        greet(dev(sx, z, c))
        greet(dev(sy, z, c))
    else:
        for i in range(1, spots):
            greet(dev(lax.rem(s + i, spots), z, c))
    greet(here)

    def remote(src, dst, ss, rs, where):
        return pltpu.make_async_remote_copy(
            src_ref=src, dst_ref=dst, send_sem=ss, recv_sem=rs,
            device_id=where, device_id_type=pl.DeviceIdType.MESH)

    def each(copies, what):
        for p in copies:
            getattr(p, what)()

    def own_tok(u):
        cols = pl.ds(pl.multiple_of((u * CORES + c) * rows, 128), rows)
        return pltpu.make_async_copy(tok.at[0, :, cols], tokens.at[0, u], own_s.at[u])

    def part_tok(u):
        cols = pl.ds(pl.multiple_of((u * CORES + 1 - c) * rows, 128), rows)
        return remote(tok.at[0, :, cols], tokens.at[1, u], tok_s.at[u], tok_r.at[u], here)

    own_w = [pltpu.make_async_copy(wl, wlat.at[z], own_s.at[planes]),
             pltpu.make_async_copy(wr, wrope.at[z], own_s.at[planes + 1])]
    each(own_w, "start")
    place = pl.ds(pl.multiple_of(s * span, 128), span)
    loads = [(kup, kbuf), (vup, vbuf), (cos_hbm.at[:, place], cos_ref), (sin_hbm.at[:, place], sin_ref),
             (cosq_hbm, cosq), (sinq_hbm, sinq), (scale_hbm, scale), (q_hbm, qbuf)]
    loads = [pltpu.make_async_copy(a, b, up_s.at[i]) for i, (a, b) in enumerate(loads)]
    each(loads, "start")
    for u in range(planes):
        own_tok(u).start()
    each(own_w, "wait")
    pl.semaphore_wait(barrier, (2 if near else spots - 1) + 1 + has_up.astype(jnp.int32) + has_down.astype(jnp.int32))

    def block(u, of, k, ss, rs, where):
        rng = pl.ds(pl.multiple_of(of * quarter + k * eighth, 16), eighth)
        out = [remote(wlat.at[u, rng], wlat.at[u, rng], ss(k), rs(k), where)]
        if k == 0:
            rng = pl.ds(pl.multiple_of(of * rpart, 16), rpart)
            out.append(remote(wrope.at[u, rng], wrope.at[u, rng], ss(2), rs(2), where))
        return out

    def extra(u):
        hops = jnp.where((u > z) | ((u == z) & ~has_up), u, planes - 1 - u)
        return jnp.where(hops == planes - 1, 2, 1)

    def extra_to(u, up_way):
        hops = planes - 1 - u if up_way else u
        return jnp.where(hops == planes - 1, 2, 1)

    def z_block(u, k, ss, where):
        if k < 2:
            return block(u, q, k, ss, lambda i: z_r.at[i, u], where)
        return block(u, qd, 3 - k, lambda i: ss(3 + i), lambda i: z_r.at[3 + i, u], where)

    def z_up(u, k):
        return z_block(u, k, lambda i: zu_s.at[i, u], dev(s, z + 1, c))

    def z_down(u, k):
        return z_block(u, k, lambda i: zd_s.at[i, u], dev(s, z - 1, c))

    def z_in(u, k):
        return z_block(u, k, lambda i: zu_s.at[i, u], here)

    def sent(u, k, up_way):
        return k < 3 or extra_to(u, up_way) == 2

    def by_y(u):
        return (u + c) % 2 == 0

    def piece(u, of, k, ss, rs, where):
        return block(u, of, k, lambda i: ss.at[i, u], lambda i: rs.at[i, u], where)

    def x_copy(u, k):
        return piece(u, q, k, x_s, x_r, dev(sx, z, c))

    def y_copy(u, k):
        return piece(u, q, k, y_s, y_r, dev(sy, z, c))

    def x_in(u, k):
        return piece(u, qx, k, x_s, x_r, here)

    def y_in(u, k):
        return piece(u, qy, k, y_s, y_r, here)

    def relay(u, of, where):
        return block(u, of, 0, lambda i: d_s.at[i // 2, u], lambda i: d_r.at[i // 2, u], where)

    def dy_copy(u):
        return relay(u, qx, dev(sy, z, c))

    def dx_copy(u):
        return relay(u, qy, dev(sx, z, c))

    def d_in(u):
        return relay(u, qd, here)

    for k in range(4):
        @pl.when(has_up & sent(z, k, True))
        def _():
            each(z_up(z, k), "start")

        @pl.when(has_down & sent(z, k, False))
        def _():
            each(z_down(z, k), "start")

    for u in range(planes):
        part_tok(u).start()
    each(loads, "wait")
    ks = kbuf[...].astype(F32)
    vs = vbuf[...].astype(F32)
    for h in range(heads):
        up[:, h * kw:(h + 1) * kw] = ks[:, h, :].astype(BF16)
        up[:, heads * kw + h * vw:heads * kw + (h + 1) * vw] = vs[:, h, :].astype(BF16)
    for b in range(CORES):
        query = qbuf[b].astype(F32)
        turned_out[b] = turn(query[:, kw:], cosq[...], sinq[...]).astype(BF16)
        tiled = jnp.concatenate([query[:, :kw]] * heads, axis=1)
        row = lax.broadcasted_iota(jnp.int32, tiled.shape, 0)
        col = lax.broadcasted_iota(jnp.int32, tiled.shape, 1)
        blocked[b] = jnp.where(col // kw == row, tiled, 0.0).astype(BF16)
    contract = (((1,), (1,)), ((), ()))

    def block_dot(u):
        x = tokens[:, u].reshape(CORES * span, rows)
        return (jnp.dot(x, wlat[u], preferred_element_type=F32),
                lax.dot_general(wrope[u], x, contract, preferred_element_type=F32))

    def valid(u):
        return (u >= 0) & (u < planes)

    def relayed(u):
        return (u != z) & (extra(u) == 1)

    def step(d, carry):
        for k in range(4):
            for sign in (-1, 1):
                u = z + sign * d

                @pl.when(valid(u) & sent(u, k, sign < 0))
                def _():
                    each(z_in(u, k), "wait_recv")
                    if sign < 0:
                        @pl.when(has_up)
                        def _():
                            each(z_up(u, k), "start")
                    else:
                        @pl.when(has_down)
                        def _():
                            each(z_down(u, k), "start")
                    if k < 2:
                        each(x_copy(u, k), "start")
                        each(y_copy(u, k), "start")
            if k == 0:
                for sign in (-1, 1):
                    u = z + sign * (d - 1)

                    @pl.when(valid(u) & (d > 1) & relayed(u))
                    def _():
                        @pl.when(by_y(u))
                        def _():
                            each(x_in(u, 0), "wait_recv")
                            each(dy_copy(u), "start")

                        @pl.when(~by_y(u))
                        def _():
                            each(y_in(u, 0), "wait_recv")
                            each(dx_copy(u), "start")
            if k == 1:
                @pl.when(d == 1)
                def _():
                    for u in range(planes):
                        own_tok(u).wait()
                        part_tok(u).wait()
                    a, b = block_dot(z)
                    acc[...] = a
                    acct[...] = b

                for sign in (-1, 1):
                    u = z + sign * (d - 2)

                    @pl.when(valid(u) & (d > 2))
                    def _():
                        @pl.when(~relayed(u) | ~by_y(u))
                        def _():
                            each(x_in(u, 0), "wait_recv")

                        @pl.when(~relayed(u) | by_y(u))
                        def _():
                            each(y_in(u, 0), "wait_recv")

                        each(x_in(u, 1), "wait_recv")
                        each(y_in(u, 1), "wait_recv")

                        @pl.when(relayed(u))
                        def _():
                            each(d_in(u), "wait_recv")
                        a, b = block_dot(u)
                        acc[...] += a
                        acct[...] += b
        return carry

    lax.fori_loop(1, planes + 2, step, 0)

    swaps = [remote(acc.at[pl.ds(span, span)], other, acc_s.at[0], acc_r.at[0], here),
             remote(acct.at[:, pl.ds(span, span)], othert, acc_s.at[1], acc_r.at[1], here)]
    each(swaps, "start")
    each(swaps, "wait")
    latent = acc[:span] + other[...]
    ropes = acct[:, :span] + othert[...]
    scaled = latent * lax.rsqrt(jnp.mean(latent * latent, axis=-1, keepdims=True) + 1e-06)
    spread[z] = (scaled * scale[...]).astype(BF16)
    swapped = jnp.concatenate([ropes[rope // 2:], ropes[:rope // 2]], axis=0)
    spreadt[z] = (ropes * cos_ref[...] + swapped * sin_ref[...]).astype(BF16)

    def cut(k):
        return pl.ds(pl.multiple_of(k * part, 16), part)

    def lanes(si):
        return pl.ds(pl.multiple_of(si * span, 128), span)

    def act(k, main, turned, what):
        getattr(main, what)()

        @pl.when(k == 0)
        def _():
            getattr(turned, what)()

    def g_copy(u, k, zi, slot, what):
        act(k, remote(spread.at[u, cut(k)], spread.at[u, cut(k)], g_s.at[slot, k, u], g_r.at[k, u], dev(s, zi, c)),
            remote(spreadt.at[u], spreadt.at[u], g_s.at[slot, PARTS, u], g_r.at[PARTS, u], dev(s, zi, c)), what)

    def f_copy(u, k, where, si, what):
        act(k, remote(spread.at[u, cut(k)], xall.at[c, si, cut(k)], f_s.at[k, u], f_r.at[k, si], where),
            remote(spreadt.at[u], rot_out.at[c, :, lanes(si)], f_s.at[PARTS, u], f_r.at[PARTS, si], where), what)

    def b_copy(u, k, what):
        where = dev(jnp.where(k < 2, sx, sy), z, c)
        act(k, remote(spread.at[u, cut(k)], between.at[cut(k)], f_s.at[k, u], m_r.at[k], where),
            remote(spreadt.at[u], betweent, f_s.at[PARTS, u], m_r.at[PARTS], where), what)

    def m_copy(k, what):
        si = jnp.where(k < 2, sx, sy)
        where = dev(jnp.where(k < 2, sy, sx), z, c)
        act(k, remote(between.at[cut(k)], xall.at[c, si, cut(k)], m_s.at[k], f_r.at[k, si], where),
            remote(betweent, rot_out.at[c, :, lanes(si)], m_s.at[PARTS], f_r.at[PARTS, si], where), what)

    def p_own(k, what):
        act(k, remote(spread.at[s, cut(k)], xall.at[c, s, cut(k)], p_s.at[k, s], p_r.at[k, s], here),
            remote(spreadt.at[s], rot_out.at[c, :, lanes(s)], p_s.at[PARTS, s], p_r.at[PARTS, s], here), what)

    def p_copy(ci, si, k, what):
        turned = rot_out.at[ci, :, lanes(si)]
        act(k, remote(xall.at[ci, si, cut(k)], xall.at[ci, si, cut(k)], p_s.at[k, si], p_r.at[k, si], here),
            remote(turned, turned, p_s.at[PARTS, si], p_r.at[PARTS, si], here), what)

    def deliver(u, k):
        if near:
            @pl.when((u != s) & (u != sd))
            def _():
                f_copy(u, k, dev(u, z, c), s, "start")

            @pl.when(u == sd)
            def _():
                b_copy(u, k, "start")
        else:
            @pl.when(u != s)
            def _():
                f_copy(u, k, dev(u, z, c), s, "start")

        @pl.when(u == s)
        def _():
            p_own(k, "start")

    def gone(u, what):
        def one(k, carry):
            @pl.when(u != s)
            def _():
                f_copy(u, k, here, s, what)

            @pl.when((u <= z) & ups(u))
            def _():
                g_copy(u, k, z, 0, what)

            @pl.when((u >= z) & downs(u))
            def _():
                g_copy(u, k, z, 1, what)
            return carry
        lax.fori_loop(0, PARTS, one, 0)

    jump = planes > 2
    across = jump & ((z == 0) | (z == planes - 1))
    end = planes - 1 - z

    def g_jump(k, what):
        act(k, remote(spread.at[z, cut(k)], spread.at[z, cut(k)], j_s.at[k], g_r.at[k, z], dev(s, end, c)),
            remote(spreadt.at[z], spreadt.at[z], j_s.at[PARTS], g_r.at[PARTS, z], dev(s, end, c)), what)

    if jump:
        @pl.when(across)
        def _():
            def far(k, carry):
                g_jump(k, "start")
                return carry

            lax.fori_loop(0, PARTS, far, 0)

    def first(k, carry):
        @pl.when(has_up)
        def _():
            g_copy(z, k, z + 1, 0, "start")

        @pl.when(has_down)
        def _():
            g_copy(z, k, z - 1, 1, "start")
        return carry

    lax.fori_loop(0, PARTS, first, 0)

    def second(k, carry):
        deliver(z, k)
        return carry

    lax.fori_loop(0, PARTS, second, 0)

    def drain(u, carry):
        for k in range(4):
            @pl.when((u >= z) & has_down & sent(u, k, False))
            def _():
                each(z_down(u, k), "wait_send")

            @pl.when((u <= z) & has_up & sent(u, k, True))
            def _():
                each(z_up(u, k), "wait_send")

        for k in range(2):
            @pl.when(u != z)
            def _():
                each(x_copy(u, k), "wait_send")
                each(y_copy(u, k), "wait_send")

        @pl.when(relayed(u))
        def _():
            each(dy_copy(u), "wait_send")
        return carry

    lax.fori_loop(0, planes, drain, 0)

    def fill(ci, si, x):
        keys = jnp.dot(x, up[:, :heads * kw], preferred_element_type=F32)
        values = jnp.dot(x, up[:, heads * kw:], preferred_element_type=F32)
        where = pl.ds(pl.multiple_of(si * span * heads, 128), span * heads)
        for h in range(heads):
            wide[0, pl.ds(h, span, stride=heads), :] = keys[:, h * kw:(h + 1) * kw]
        k_out[ci, where, :] = wide[0].astype(BF16)
        for h in range(heads):
            wide[1, pl.ds(h, span, stride=heads), :] = values[:, h * vw:(h + 1) * vw]
        v_out[ci, where, :] = wide[1].astype(BF16)
        flat_out[ci, lanes(si), :] = values.astype(BF16)
        score_out[ci, :, lanes(si)] = lax.dot_general(blocked[ci], keys.astype(BF16), contract, preferred_element_type=F32)

    inner = z < planes // 2
    edge = (z == 0) | (z == planes - 1)
    pace = jnp.where(edge, PARTS, 2 * PARTS)

    def ups(u):
        return has_up & ((u > 0) | (z + 1 < planes - 1) | (z == 0))

    def downs(u):
        return has_down & ((u < planes - 1) | (z > 1) | (z == planes - 1))

    def begin(u):
        far = jnp.where(u > z, u - z, z - u)
        side = jnp.where((u > z) == inner, 0, PARTS)
        return jnp.where(u == z, -LAG, pace * (far - 1) + side)

    last = max(PARTS * (planes - 2), 2 * PARTS * (planes - 3) + PARTS) + PARTS + LAG - 1

    def go(n, carry):
        for toward in (True, False):
            i = n if toward else n - PARTS
            d = lax.div(i, pace) + 1
            k = lax.rem(i, pace)
            up_way = ~inner if toward else inner
            u = jnp.where(up_way, z - d, z + d)

            @pl.when(valid(u) & (i >= 0) & (k < PARTS))
            def _():
                g_copy(u, k, z, 0, "wait_recv")

                @pl.when(up_way & ups(u))
                def _():
                    g_copy(u, k, z + 1, 0, "start")

                @pl.when(~up_way & downs(u))
                def _():
                    g_copy(u, k, z - 1, 1, "start")
                deliver(u, k)

        def arrive(k, si):
            f_copy(0, k, here, si, "wait_recv")
            p_copy(c, si, k, "start")

        k = n - begin(s) - LAG
        if near:
            @pl.when((k >= 0) & (k < PARTS))
            def _():
                arrive(k, sx)
                arrive(k, sy)

            kx = n - begin(sy) - LAG

            @pl.when((kx >= 0) & (kx < 2))
            def _():
                m_wait(kx)
                m_copy(kx, "start")

            ky = n - begin(sx) - LAG

            @pl.when((ky >= 2) & (ky < PARTS))
            def _():
                m_wait(ky)
                m_copy(ky, "start")

            kd = k - 3

            @pl.when((kd >= 0) & (kd < PARTS))
            def _():
                arrive(kd, sd)
        else:
            @pl.when((k >= 0) & (k < PARTS))
            def _():
                def other_spot(i, carry):
                    arrive(k, lax.rem(s + i, spots))
                    return carry
                lax.fori_loop(1, spots, other_spot, 0)

        i = n - last

        if near:
            i = jnp.where(n >= last + 4, n - last - 1, jnp.where(n == last + 3, spots, i))

        @pl.when((i >= 0) & (i < spots))
        def _():
            if near:
                si = jnp.where(i == 0, s, jnp.where(i == 1, sx, jnp.where(i == 2, sy, sd)))
            else:
                si = lax.rem(s + i, spots)

            @pl.when(i == 0)
            def _():
                rot_out[c, :, lanes(s)] = spreadt[s]
                xall[c, s] = spread[s]

            fill(c, si, xall[c, si])

            def landed(k, carry):
                p_copy(1 - c, si, k, "wait_recv")
                return carry

            lax.fori_loop(0, PARTS, landed, 0)
            fill(1 - c, si, xall[1 - c, si])
        return carry

    def m_wait(k):
        act(k, remote(between.at[cut(k)], between.at[cut(k)], m_s.at[k], m_r.at[k], here),
            remote(betweent, betweent, m_s.at[PARTS], m_r.at[PARTS], here), "wait_recv")

    lax.fori_loop(0, last + spots + (1 if near else 0), go, 0)

    def leave(u, carry):
        gone(u, "wait_send")

        def one(k, carry):
            p_copy(c, u, k, "wait_send")
            return carry

        lax.fori_loop(0, PARTS, one, 0)
        return carry

    lax.fori_loop(0, planes, leave, 0)

    def ended(k, carry):
        if near:
            m_copy(k, "wait_send")
        if jump:
            @pl.when(across)
            def _():
                g_jump(k, "wait_send")
        return carry

    lax.fori_loop(0, PARTS, ended, 0)


def read_kernel(k_ref, v_ref, flat_ref, score_ref, rot_ref, turned_ref, plain_hbm, value_hbm, rot_hbm, read_hbm, reads, sems):
    heads, length = score_ref.shape[1:]
    kw = k_ref.shape[2]
    vw = v_ref.shape[2]
    rope = rot_ref.shape[1]
    copies = [pltpu.make_async_copy(a, b, sems.at[i])
              for i, (a, b) in enumerate([(k_ref, plain_hbm), (v_ref, value_hbm), (rot_ref, rot_hbm)])]
    for copy in copies:
        copy.start()
    for b in range(CORES):
        scores = score_ref[b] + jnp.dot(turned_ref[b], rot_ref[b], preferred_element_type=F32)
        scores = scores * (1.0 / (kw + rope) ** 0.5)
        weights = jnp.exp(scores - jnp.max(scores, axis=-1, keepdims=True))
        total = jnp.sum(weights, axis=-1, keepdims=True)
        mixed = jnp.dot(weights.astype(BF16), flat_ref[b], preferred_element_type=F32) / total
        for h in range(heads):
            reads[b, h:h + 1, :] = mixed[h:h + 1, h * vw:(h + 1) * vw].astype(BF16)
    last = pltpu.make_async_copy(reads, read_hbm, sems.at[3])
    last.start()
    for copy in copies:
        copy.wait()
    last.wait()


def body(planes, spots, tokens, latent_down, rope_weight, norm_scale, key_up, value_up, query):
    span = tokens.shape[1]
    rows, lat = latent_down.shape
    rope = rope_weight.shape[1]
    heads, kw = key_up.shape[1:]
    vw = value_up.shape[2]
    length = spots * span
    cosine, sine = turn_tables(np.arange(length + 1), rope)
    vmem = pl.BlockSpec(memory_space=pltpu.VMEM)
    hbm = pl.BlockSpec(memory_space=pltpu.HBM)
    dma = pltpu.SemaphoreType.DMA
    operands = (tokens, latent_down, rope_weight.T, norm_scale.reshape(1, lat),
                jnp.asarray(np.ascontiguousarray(cosine[:length].T)), jnp.asarray(np.ascontiguousarray(sine[:length].T)),
                jnp.asarray(cosine[length:]), jnp.asarray(sine[length:]), key_up, value_up, query)
    results = pl.pallas_call(
        functools.partial(move_kernel, planes, spots),
        out_shape=(pltpu.VMEM((CORES, length * heads, kw), BF16),
                   pltpu.VMEM((CORES, length * heads, vw), BF16),
                   pltpu.VMEM((CORES, length, heads * vw), BF16),
                   pltpu.VMEM((CORES, heads, length), F32),
                   pltpu.VMEM((CORES, rope, length), BF16),
                   pltpu.VMEM((CORES, heads, rope), BF16)),
        in_specs=[hbm] * len(operands),
        out_specs=(vmem,) * 6,
        scratch_shapes=[
            pltpu.VMEM((CORES, planes, span, rows), BF16),
            pltpu.VMEM((planes, rows, lat), BF16),
            pltpu.VMEM((planes, rope, rows), BF16),
            pltpu.VMEM((CORES * span, lat), F32),
            pltpu.VMEM((rope, CORES * span), F32),
            pltpu.VMEM((span, lat), F32),
            pltpu.VMEM((rope, span), F32),
            pltpu.VMEM((planes, span, lat), BF16),
            pltpu.VMEM((planes, rope, span), BF16),
            pltpu.VMEM((CORES, spots, span, lat), BF16),
            pltpu.VMEM((span, lat), BF16),
            pltpu.VMEM((rope, span), BF16),
            pltpu.VMEM(key_up.shape, BF16),
            pltpu.VMEM(value_up.shape, BF16),
            pltpu.VMEM((lat, heads * (kw + vw)), BF16),
            pltpu.VMEM(query.shape, BF16),
            pltpu.VMEM((CORES, heads, heads * kw), BF16),
            pltpu.VMEM((2, span * heads, kw), F32),
            pltpu.VMEM((rope, span), F32),
            pltpu.VMEM((rope, span), F32),
            pltpu.VMEM((1, rope), F32),
            pltpu.VMEM((1, rope), F32),
            pltpu.VMEM((1, lat), F32),
            dma((planes,)), dma((planes,)), dma((planes + 2,)),
            dma((6, planes)), dma((6, planes)), dma((6, planes)),
            dma((3, planes)), dma((3, planes)), dma((3, planes)), dma((3, planes)),
            dma((2, planes)), dma((2, planes)),
            dma((2,)), dma((2,)),
            dma((2, PARTS + 1, planes)), dma((PARTS + 1, planes)), dma((PARTS + 1,)),
            dma((PARTS + 1, planes)), dma((PARTS + 1, spots)),
            dma((PARTS + 1,)), dma((PARTS + 1,)),
            dma((PARTS + 1, spots)), dma((PARTS + 1, spots)),
            dma((8,)),
        ],
        compiler_params=pltpu.CompilerParams(collective_id=0, has_side_effects=True, vmem_limit_bytes=VMEM_BYTES),
    )(*[pltpu.with_memory_space_constraint(v, pltpu.HBM) for v in operands])
    plain, value, rot, read = pl.pallas_call(
        read_kernel,
        out_shape=(jax.ShapeDtypeStruct((CORES, length * heads, kw), BF16),
                   jax.ShapeDtypeStruct((CORES, length * heads, vw), BF16),
                   jax.ShapeDtypeStruct((CORES, rope, length), BF16),
                   jax.ShapeDtypeStruct((CORES, heads, vw), BF16)),
        in_specs=[vmem] * 6,
        out_specs=(hbm,) * 4,
        scratch_shapes=[pltpu.VMEM((CORES, heads, vw), BF16), dma((4,))],
        compiler_params=pltpu.CompilerParams(vmem_limit_bytes=VMEM_BYTES // 2),
    )(*results)
    return (plain.reshape(CORES, length, heads, kw), value.reshape(CORES, length, heads, vw), jnp.swapaxes(rot, 1, 2), read)


def solution(mesh):
    planes = mesh.shape["tp"] // CORES
    spots = mesh.shape["sp"]
    assert planes == spots and spots % 4 == 0
    in_specs = (
        P("tp", "sp", None),
        P("tp", None),
        P("tp", None),
        P(),
        P(None, "tp", None),
        P(None, "tp", None),
        P("sp", "tp", None),
    )
    out_specs = (
        P("sp", None, "tp", None),
        P("sp", None, "tp", None),
        P("sp", None, None),
        P("sp", "tp", None),
    )
    return jax.shard_map(functools.partial(body, planes, spots), mesh=mesh, in_specs=in_specs,
                         out_specs=out_specs, check_vma=False)
```

time: 54.9 us -> 49.2 us (0.90)
  the two profiles are of different devices: /device:TPU:7 before, /device:TPU:6 now
where the time goes in v1:
time: 49.2 us; the launch traced here: 49.1 us
  Pallas kernels  48.4 us (98%)
  between operations  0.64 us (1%)
    pallas_call x1, Pallas kernels, body(): pl.pallas_call(functools.partial(move_kernel, planes, spots), out_shape=(...  47 us
    pallas_call x1, Pallas kernels, body(): pl.pallas_call(read_kernel, out_shape=(jax.ShapeDtypeStruct((CORES, lengt...  1.4 us

profile of v1, /device:TPU:6, one launch (start us, length us, event | category | flops | bytes accessed | tf_op | source)
XLA Modules:
  0.0 49.1 jit_solution(3147475828980687126)
XLA Ops:
  0.6 47.0 %shard_map.138 = (bf16[2,2048,128]{2,1,0:T(8,128)(2,1)S(1)}, bf16[2,2048,128]{2,1,0:T(8,128)(2,1)S(1)}, bf16[2,512,512]{2,1,0:T(8,128)(2,1)S(1)}, f32[2,4,512]{2...) custom-call(bf16[1,128,4096]{2,1,0:T(8,128)(2,1)} %tok.1, bf16[512,512]{1,0:T(8,128)(2,1)} %wl.1, ...), custom_call_target="tpu_custom_call" | custom-call | tf_op jit(solution)/shard_map/pallas_call | solution.py:617
  47.7 1.4 %shard_map.139 = (bf16[2,2048,128]{2,1,0:T(8,128)(2,1)}, bf16[2,2048,128]{2,1,0:T(8,128)(2,1)}, bf16[2,64,512]{2,1,0:T(8,128)(2,1)}, bf16[2,4,128]{2,1,0:T(4,128)(2,1)}) custom-call(bf16[2,2048,128]{2,1,0:T(8,128)(2,1)S(1)} %get-tuple-element.14.k_ref, bf16[2,2048,128]{2,1,0:T(8,128)(2,1)S(1)} %get-tuple-element.15.v_ref, ...), custom_call_target="tpu_custom_call" | custom-call | tf_op jit(solution)/shard_map/pallas_call | solution.py:664

commit v2 on v1

--- a/solution.py
+++ b/solution.py
@@ -35,7 +35,7 @@
                 k_out, v_out, flat_out, score_out, rot_out, turned_out,
                 tokens, wlat, wrope, acc, acct, other, othert, spread, spreadt, xall, between, betweent,
                 kbuf, vbuf, up, qbuf, blocked, wide, cos_ref, sin_ref, cosq, sinq, scale,
-                tok_s, tok_r, own_s, zu_s, zd_s, z_r, x_s, x_r, y_s, y_r, d_s, d_r,
+                tok_s, own_s, zu_s, zd_s, z_r, x_s, x_r, y_s, y_r, d_s, d_r,
                 acc_s, acc_r, g_s, g_r, j_s, f_s, f_r, m_s, m_r, p_s, p_r, up_s):
     s = lax.axis_index("sp")
     t = lax.axis_index("tp")
@@ -97,14 +97,14 @@
 
     def own_tok(u):
         cols = pl.ds(pl.multiple_of((u * CORES + c) * rows, 128), rows)
-        return pltpu.make_async_copy(tok.at[0, :, cols], tokens.at[0, u], own_s.at[u])
+        return pltpu.make_async_copy(tok.at[0, :, cols], tokens.at[0, u], own_s.at[0])
 
     def part_tok(u):
         cols = pl.ds(pl.multiple_of((u * CORES + 1 - c) * rows, 128), rows)
-        return remote(tok.at[0, :, cols], tokens.at[1, u], tok_s.at[u], tok_r.at[u], here)
-
-    own_w = [pltpu.make_async_copy(wl, wlat.at[z], own_s.at[planes]),
-             pltpu.make_async_copy(wr, wrope.at[z], own_s.at[planes + 1])]
+        return remote(tok.at[0, :, cols], tokens.at[1, u], tok_s.at[0], tok_s.at[1], here)
+
+    own_w = [pltpu.make_async_copy(wl, wlat.at[z], own_s.at[1]),
+             pltpu.make_async_copy(wr, wrope.at[z], own_s.at[2])]
     each(own_w, "start")
     place = pl.ds(pl.multiple_of(s * span, 128), span)
     loads = [(kup, kbuf), (vup, vbuf), (cos_hbm.at[:, place], cos_ref), (sin_hbm.at[:, place], sin_ref),
@@ -135,16 +135,16 @@
     def z_block(u, k, ss, where):
         if k < 2:
             return block(u, q, k, ss, lambda i: z_r.at[i, u], where)
-        return block(u, qd, 3 - k, lambda i: ss(3 + i), lambda i: z_r.at[3 + i, u], where)
+        return block(u, qd, 3 - k, ss, lambda i: z_r.at[3 + i, u], where)
 
     def z_up(u, k):
-        return z_block(u, k, lambda i: zu_s.at[i, u], dev(s, z + 1, c))
+        return z_block(u, k, lambda i: zu_s.at[i // 2, u], dev(s, z + 1, c))
 
     def z_down(u, k):
-        return z_block(u, k, lambda i: zd_s.at[i, u], dev(s, z - 1, c))
+        return z_block(u, k, lambda i: zd_s.at[i // 2, u], dev(s, z - 1, c))
 
     def z_in(u, k):
-        return z_block(u, k, lambda i: zu_s.at[i, u], here)
+        return z_block(u, k, lambda i: zu_s.at[i // 2, u], here)
 
     def sent(u, k, up_way):
         return k < 3 or extra_to(u, up_way) == 2
@@ -152,20 +152,17 @@
     def by_y(u):
         return (u + c) % 2 == 0
 
-    def piece(u, of, k, ss, rs, where):
-        return block(u, of, k, lambda i: ss.at[i, u], lambda i: rs.at[i, u], where)
-
     def x_copy(u, k):
-        return piece(u, q, k, x_s, x_r, dev(sx, z, c))
+        return block(u, q, k, lambda i: x_s.at[i // 2], lambda i: x_r.at[i, u], dev(sx, z, c))
 
     def y_copy(u, k):
-        return piece(u, q, k, y_s, y_r, dev(sy, z, c))
+        return block(u, q, k, lambda i: y_s.at[i // 2], lambda i: y_r.at[i, u], dev(sy, z, c))
 
     def x_in(u, k):
-        return piece(u, qx, k, x_s, x_r, here)
+        return block(u, qx, k, lambda i: x_s.at[i // 2], lambda i: x_r.at[i, u], here)
 
     def y_in(u, k):
-        return piece(u, qy, k, y_s, y_r, here)
+        return block(u, qy, k, lambda i: y_s.at[i // 2], lambda i: y_r.at[i, u], here)
 
     def relay(u, of, where):
         return block(u, of, 0, lambda i: d_s.at[i // 2, u], lambda i: d_r.at[i // 2, u], where)
@@ -253,9 +250,8 @@
             if k == 1:
                 @pl.when(d == 1)
                 def _():
-                    for u in range(planes):
-                        own_tok(u).wait()
-                        part_tok(u).wait()
+                    pltpu.make_async_copy(tokens.at[0], tokens.at[0], own_s.at[0]).wait()
+                    remote(tokens.at[1], tokens.at[1], tok_s.at[0], tok_s.at[1], here).wait()
                     a, b = block_dot(z)
                     acc[...] = a
                     acct[...] = b
@@ -311,32 +307,32 @@
             getattr(turned, what)()
 
     def g_copy(u, k, zi, slot, what):
-        act(k, remote(spread.at[u, cut(k)], spread.at[u, cut(k)], g_s.at[slot, k, u], g_r.at[k, u], dev(s, zi, c)),
-            remote(spreadt.at[u], spreadt.at[u], g_s.at[slot, PARTS, u], g_r.at[PARTS, u], dev(s, zi, c)), what)
+        act(k, remote(spread.at[u, cut(k)], spread.at[u, cut(k)], g_s.at[0, slot, u], g_r.at[k, u], dev(s, zi, c)),
+            remote(spreadt.at[u], spreadt.at[u], g_s.at[1, slot, u], g_r.at[PARTS, u], dev(s, zi, c)), what)
 
     def f_copy(u, k, where, si, what):
-        act(k, remote(spread.at[u, cut(k)], xall.at[c, si, cut(k)], f_s.at[k, u], f_r.at[k, si], where),
-            remote(spreadt.at[u], rot_out.at[c, :, lanes(si)], f_s.at[PARTS, u], f_r.at[PARTS, si], where), what)
+        act(k, remote(spread.at[u, cut(k)], xall.at[c, si, cut(k)], f_s.at[0], f_r.at[k, si], where),
+            remote(spreadt.at[u], rot_out.at[c, :, lanes(si)], f_s.at[1], f_r.at[PARTS, si], where), what)
 
     def b_copy(u, k, what):
         where = dev(jnp.where(k < 2, sx, sy), z, c)
-        act(k, remote(spread.at[u, cut(k)], between.at[cut(k)], f_s.at[k, u], m_r.at[k], where),
-            remote(spreadt.at[u], betweent, f_s.at[PARTS, u], m_r.at[PARTS], where), what)
+        act(k, remote(spread.at[u, cut(k)], between.at[cut(k)], f_s.at[0], m_r.at[k], where),
+            remote(spreadt.at[u], betweent, f_s.at[1], m_r.at[PARTS], where), what)
 
     def m_copy(k, what):
         si = jnp.where(k < 2, sx, sy)
         where = dev(jnp.where(k < 2, sy, sx), z, c)
-        act(k, remote(between.at[cut(k)], xall.at[c, si, cut(k)], m_s.at[k], f_r.at[k, si], where),
-            remote(betweent, rot_out.at[c, :, lanes(si)], m_s.at[PARTS], f_r.at[PARTS, si], where), what)
+        act(k, remote(between.at[cut(k)], xall.at[c, si, cut(k)], m_s.at[0], f_r.at[k, si], where),
+            remote(betweent, rot_out.at[c, :, lanes(si)], m_s.at[1], f_r.at[PARTS, si], where), what)
 
     def p_own(k, what):
-        act(k, remote(spread.at[s, cut(k)], xall.at[c, s, cut(k)], p_s.at[k, s], p_r.at[k, s], here),
-            remote(spreadt.at[s], rot_out.at[c, :, lanes(s)], p_s.at[PARTS, s], p_r.at[PARTS, s], here), what)
+        act(k, remote(spread.at[s, cut(k)], xall.at[c, s, cut(k)], p_s.at[0], p_r.at[0, s], here),
+            remote(spreadt.at[s], rot_out.at[c, :, lanes(s)], p_s.at[1], p_r.at[1, s], here), what)
 
     def p_copy(ci, si, k, what):
         turned = rot_out.at[ci, :, lanes(si)]
-        act(k, remote(xall.at[ci, si, cut(k)], xall.at[ci, si, cut(k)], p_s.at[k, si], p_r.at[k, si], here),
-            remote(turned, turned, p_s.at[PARTS, si], p_r.at[PARTS, si], here), what)
+        act(k, remote(xall.at[ci, si, cut(k)], xall.at[ci, si, cut(k)], p_s.at[0], p_r.at[0, si], here),
+            remote(turned, turned, p_s.at[1], p_r.at[1, si], here), what)
 
     def deliver(u, k):
         if near:
@@ -356,29 +352,13 @@
         def _():
             p_own(k, "start")
 
-    def gone(u, what):
-        def one(k, carry):
-            @pl.when(u != s)
-            def _():
-                f_copy(u, k, here, s, what)
-
-            @pl.when((u <= z) & ups(u))
-            def _():
-                g_copy(u, k, z, 0, what)
-
-            @pl.when((u >= z) & downs(u))
-            def _():
-                g_copy(u, k, z, 1, what)
-            return carry
-        lax.fori_loop(0, PARTS, one, 0)
-
     jump = planes > 2
     across = jump & ((z == 0) | (z == planes - 1))
     end = planes - 1 - z
 
     def g_jump(k, what):
-        act(k, remote(spread.at[z, cut(k)], spread.at[z, cut(k)], j_s.at[k], g_r.at[k, z], dev(s, end, c)),
-            remote(spreadt.at[z], spreadt.at[z], j_s.at[PARTS], g_r.at[PARTS, z], dev(s, end, c)), what)
+        act(k, remote(spread.at[z, cut(k)], spread.at[z, cut(k)], j_s.at[0], g_r.at[k, z], dev(s, end, c)),
+            remote(spreadt.at[z], spreadt.at[z], j_s.at[1], g_r.at[PARTS, z], dev(s, end, c)), what)
 
     if jump:
         @pl.when(across)
@@ -407,21 +387,24 @@
 
     lax.fori_loop(0, PARTS, second, 0)
 
+    def left(ref, sem):
+        remote(ref, ref, sem, sem, here).wait_send()
+
+    def left_z(u, sems, up_way):
+        for n in (1, 2):
+            @pl.when(extra_to(u, up_way) == n)
+            def _():
+                left(wlat.at[u, pl.ds(0, (2 + n) * eighth)], sems.at[0, u])
+                left(wrope.at[u, pl.ds(0, n * rpart)], sems.at[1, u])
+
     def drain(u, carry):
-        for k in range(4):
-            @pl.when((u >= z) & has_down & sent(u, k, False))
-            def _():
-                each(z_down(u, k), "wait_send")
-
-            @pl.when((u <= z) & has_up & sent(u, k, True))
-            def _():
-                each(z_up(u, k), "wait_send")
-
-        for k in range(2):
-            @pl.when(u != z)
-            def _():
-                each(x_copy(u, k), "wait_send")
-                each(y_copy(u, k), "wait_send")
+        @pl.when((u >= z) & has_down)
+        def _():
+            left_z(u, zd_s, False)
+
+        @pl.when((u <= z) & has_up)
+        def _():
+            left_z(u, zu_s, True)
 
         @pl.when(relayed(u))
         def _():
@@ -429,6 +412,9 @@
         return carry
 
     lax.fori_loop(0, planes, drain, 0)
+    for sems in (x_s, y_s):
+        left(wlat.at[pl.ds(0, planes - 1), pl.ds(0, quarter)], sems.at[0])
+        left(wrope.at[pl.ds(0, planes - 1), pl.ds(0, rpart)], sems.at[1])
 
     def fill(ci, si, x):
         keys = jnp.dot(x, up[:, :heads * kw], preferred_element_type=F32)
@@ -445,7 +431,9 @@
 
     inner = z < planes // 2
     edge = (z == 0) | (z == planes - 1)
-    pace = jnp.where(edge, PARTS, 2 * PARTS)
+    turns = 2 * PARTS
+    rim_end = PARTS * max(planes - 3, 0)
+    core_end = turns * (planes - 2) - PARTS
 
     def ups(u):
         return has_up & ((u > 0) | (z + 1 < planes - 1) | (z == 0))
@@ -455,20 +443,30 @@
 
     def begin(u):
         far = jnp.where(u > z, u - z, z - u)
-        side = jnp.where((u > z) == inner, 0, PARTS)
-        return jnp.where(u == z, -LAG, pace * (far - 1) + side)
-
-    last = max(PARTS * (planes - 2), 2 * PARTS * (planes - 3) + PARTS) + PARTS + LAG - 1
+        rim = jnp.where(far == planes - 1, rim_end, PARTS * (far - 1))
+        near_side = jnp.where(far == 1, 0, turns * far - PARTS)
+        core = jnp.where((u > z) == inner, near_side, turns * far)
+        return jnp.where(u == z, 0, jnp.where(edge, rim, core))
+
+    last = jnp.where(edge, rim_end, core_end) + PARTS + LAG - 1
 
     def go(n, carry):
-        for toward in (True, False):
-            i = n if toward else n - PARTS
-            d = lax.div(i, pace) + 1
-            k = lax.rem(i, pace)
+        for toward in (False, True):
             up_way = ~inner if toward else inner
+            if toward:
+                rim = jnp.where(n < rim_end + PARTS, lax.div(n, PARTS) + 1, planes)
+                core = jnp.where(n < PARTS, 1, lax.div(n + PARTS, turns))
+                core = jnp.where((n >= PARTS) & (core < 2), planes, core)
+            else:
+                rim = jnp.where((n >= rim_end) & (n < rim_end + PARTS), planes - 1, planes)
+                core = jnp.where(n < turns, planes, lax.div(n, turns))
+            d = jnp.where(edge, rim, core)
+            if not toward:
+                up_way = jnp.where(edge, ~up_way, up_way)
             u = jnp.where(up_way, z - d, z + d)
-
-            @pl.when(valid(u) & (i >= 0) & (k < PARTS))
+            k = n - begin(u)
+
+            @pl.when(valid(u) & (k >= 0) & (k < PARTS))
             def _():
                 g_copy(u, k, z, 0, "wait_recv")
 
@@ -519,10 +517,10 @@
                     return carry
                 lax.fori_loop(1, spots, other_spot, 0)
 
-        i = n - last
-
         if near:
-            i = jnp.where(n >= last + 4, n - last - 1, jnp.where(n == last + 3, spots, i))
+            i = jnp.where(n == last - LAG, 0, jnp.where(n == last, 1, jnp.where(n > last + 2, n - last - 1, spots)))
+        else:
+            i = jnp.where(n == last - LAG, 0, jnp.where(n > last, n - last, spots))
 
         @pl.when((i >= 0) & (i < spots))
         def _():
@@ -538,42 +536,42 @@
 
             fill(c, si, xall[c, si])
 
-            def landed(k, carry):
-                p_copy(1 - c, si, k, "wait_recv")
-                return carry
-
-            lax.fori_loop(0, PARTS, landed, 0)
+            for ref, sem in ((xall.at[1 - c, si], p_r.at[0, si]), (rot_out.at[1 - c, :, lanes(si)], p_r.at[1, si])):
+                remote(ref, ref, sem, sem, here).wait_recv()
             fill(1 - c, si, xall[1 - c, si])
         return carry
 
     def m_wait(k):
-        act(k, remote(between.at[cut(k)], between.at[cut(k)], m_s.at[k], m_r.at[k], here),
-            remote(betweent, betweent, m_s.at[PARTS], m_r.at[PARTS], here), "wait_recv")
+        act(k, remote(between.at[cut(k)], between.at[cut(k)], m_s.at[0], m_r.at[k], here),
+            remote(betweent, betweent, m_s.at[1], m_r.at[PARTS], here), "wait_recv")
 
     lax.fori_loop(0, last + spots + (1 if near else 0), go, 0)
 
     def leave(u, carry):
-        gone(u, "wait_send")
-
-        def one(k, carry):
-            p_copy(c, u, k, "wait_send")
-            return carry
-
-        lax.fori_loop(0, PARTS, one, 0)
+        @pl.when((u <= z) & ups(u))
+        def _():
+            left(spread.at[u], g_s.at[0, 0, u])
+            left(spreadt.at[u], g_s.at[1, 0, u])
+
+        @pl.when((u >= z) & downs(u))
+        def _():
+            left(spread.at[u], g_s.at[0, 1, u])
+            left(spreadt.at[u], g_s.at[1, 1, u])
         return carry
 
     lax.fori_loop(0, planes, leave, 0)
-
-    def ended(k, carry):
-        if near:
-            m_copy(k, "wait_send")
-        if jump:
-            @pl.when(across)
-            def _():
-                g_jump(k, "wait_send")
-        return carry
-
-    lax.fori_loop(0, PARTS, ended, 0)
+    left(spread.at[pl.ds(0, planes - 1)], f_s.at[0])
+    left(spreadt.at[pl.ds(0, planes - 1)], f_s.at[1])
+    left(xall.at[0], p_s.at[0])
+    left(rot_out.at[0], p_s.at[1])
+    if near:
+        left(between, m_s.at[0])
+        left(betweent, m_s.at[1])
+    if jump:
+        @pl.when(across)
+        def _():
+            left(spread.at[z], j_s.at[0])
+            left(spreadt.at[z], j_s.at[1])
 
 
 def read_kernel(k_ref, v_ref, flat_ref, score_ref, rot_ref, turned_ref, plain_hbm, value_hbm, rot_hbm, read_hbm, reads, sems):
@@ -648,15 +646,15 @@
             pltpu.VMEM((1, rope), F32),
             pltpu.VMEM((1, rope), F32),
             pltpu.VMEM((1, lat), F32),
-            dma((planes,)), dma((planes,)), dma((planes + 2,)),
-            dma((6, planes)), dma((6, planes)), dma((6, planes)),
-            dma((3, planes)), dma((3, planes)), dma((3, planes)), dma((3, planes)),
+            dma((2,)), dma((3,)),
+            dma((2, planes)), dma((2, planes)), dma((6, planes)),
+            dma((2,)), dma((3, planes)), dma((2,)), dma((3, planes)),
             dma((2, planes)), dma((2, planes)),
             dma((2,)), dma((2,)),
-            dma((2, PARTS + 1, planes)), dma((PARTS + 1, planes)), dma((PARTS + 1,)),
-            dma((PARTS + 1, planes)), dma((PARTS + 1, spots)),
-            dma((PARTS + 1,)), dma((PARTS + 1,)),
-            dma((PARTS + 1, spots)), dma((PARTS + 1, spots)),
+            dma((2, 2, planes)), dma((PARTS + 1, planes)), dma((2,)),
+            dma((2,)), dma((PARTS + 1, spots)),
+            dma((2,)), dma((PARTS + 1,)),
+            dma((2,)), dma((2, spots)),
             dma((8,)),
         ],
         compiler_params=pltpu.CompilerParams(collective_id=0, has_side_effects=True, vmem_limit_bytes=VMEM_BYTES),

time: 49.2 us -> 45.6 us (0.927)
  the two profiles are of different devices: /device:TPU:6 before, /device:TPU:17 now
where the time goes in v2:
time: 45.6 us; the launch traced here: 45.4 us
  Pallas kernels  44.8 us (98%)
  between operations  0.64 us (1%)
    pallas_call x1, Pallas kernels, body(): pl.pallas_call(functools.partial(move_kernel, planes, spots), out_shape=(...  43.4 us
    pallas_call x1, Pallas kernels, body(): pl.pallas_call(read_kernel, out_shape=(jax.ShapeDtypeStruct((CORES, lengt...  1.4 us

profile of v2, /device:TPU:17, one launch (start us, length us, event | category | flops | bytes accessed | tf_op | source)
XLA Modules:
  0.0 45.4 jit_solution(2531238106123865989)
XLA Ops:
  0.6 43.4 %shard_map.138 = (bf16[2,2048,128]{2,1,0:T(8,128)(2,1)S(1)}, bf16[2,2048,128]{2,1,0:T(8,128)(2,1)S(1)}, bf16[2,512,512]{2,1,0:T(8,128)(2,1)S(1)}, f32[2,4,512]{2...) custom-call(bf16[1,128,4096]{2,1,0:T(8,128)(2,1)} %tok.1, bf16[512,512]{1,0:T(8,128)(2,1)} %wl.1, ...), custom_call_target="tpu_custom_call" | custom-call | tf_op jit(solution)/shard_map/pallas_call | solution.py:615
  44.0 1.4 %shard_map.139 = (bf16[2,2048,128]{2,1,0:T(8,128)(2,1)}, bf16[2,2048,128]{2,1,0:T(8,128)(2,1)}, bf16[2,64,512]{2,1,0:T(8,128)(2,1)}, bf16[2,4,128]{2,1,0:T(4,128)(2,1)}) custom-call(bf16[2,2048,128]{2,1,0:T(8,128)(2,1)S(1)} %get-tuple-element.14.k_ref, bf16[2,2048,128]{2,1,0:T(8,128)(2,1)S(1)} %get-tuple-element.15.v_ref, ...), custom_call_target="tpu_custom_call" | custom-call | tf_op jit(solution)/shard_map/pallas_call | solution.py:662

commit v3 on v2

--- a/solution.py
+++ b/solution.py
@@ -11,6 +11,7 @@
 CORES = 2
 PARTS = 4
 LAG = 4
+DLAG = 4
 VMEM_BYTES = 32 * 1024 * 1024
 BF16 = jnp.bfloat16
 F32 = jnp.float32
@@ -33,9 +34,9 @@
 
 def move_kernel(planes, spots, tok, wl, wr, scale_hbm, cos_hbm, sin_hbm, cosq_hbm, sinq_hbm, kup, vup, q_hbm,
                 k_out, v_out, flat_out, score_out, rot_out, turned_out,
-                tokens, wlat, wrope, acc, acct, other, othert, spread, spreadt, xall, between, betweent,
+                tokens, wlat, wrope, acc, acct, give, givet, other, othert, spread, spreadt, xall, between,
                 kbuf, vbuf, up, qbuf, blocked, wide, cos_ref, sin_ref, cosq, sinq, scale,
-                tok_s, own_s, zu_s, zd_s, z_r, x_s, x_r, y_s, y_r, d_s, d_r,
+                tok_s, own_s, zu_s, zd_s, z_r, xy_s, x_r, y_r, d_s, d_r,
                 acc_s, acc_r, g_s, g_r, j_s, f_s, f_r, m_s, m_r, p_s, p_r, up_s):
     s = lax.axis_index("sp")
     t = lax.axis_index("tp")
@@ -118,11 +119,32 @@
 
     def block(u, of, k, ss, rs, where):
         rng = pl.ds(pl.multiple_of(of * quarter + k * eighth, 16), eighth)
-        out = [remote(wlat.at[u, rng], wlat.at[u, rng], ss(k), rs(k), where)]
+        out = [remote(wlat.at[u, rng], wlat.at[u, rng], ss, rs, where)]
         if k == 0:
             rng = pl.ds(pl.multiple_of(of * rpart, 16), rpart)
-            out.append(remote(wrope.at[u, rng], wrope.at[u, rng], ss(2), rs(2), where))
+            out.append(remote(wrope.at[u, rng], wrope.at[u, rng], ss, rs, where))
         return out
+
+    turn_rows = rope * span // lat
+    middle = (span + turn_rows) // 2
+
+    def got(sem, ref):
+        remote(ref, ref, sem, sem, here).wait_recv()
+
+    def left(ref, sem):
+        remote(ref, ref, sem, sem, here).wait_send()
+
+    wide_rows = eighth * lat // rows
+
+    def sized(n):
+        for a in range(1, CORES + 1):
+            for b in range(1, planes + 1):
+                if n % (a * b * 8) == 0 and n // (a * b) <= span:
+                    return tokens.at[pl.ds(0, a), pl.ds(0, b), pl.ds(0, n // (a * b))]
+        raise ValueError(n)
+
+    def got_w(sem, k):
+        got(sem, sized(wide_rows + (rpart if k in (0, 3) else 0)))
 
     def extra(u):
         hops = jnp.where((u > z) | ((u == z) & ~has_up), u, planes - 1 - u)
@@ -134,17 +156,14 @@
 
     def z_block(u, k, ss, where):
         if k < 2:
-            return block(u, q, k, ss, lambda i: z_r.at[i, u], where)
-        return block(u, qd, 3 - k, ss, lambda i: z_r.at[3 + i, u], where)
+            return block(u, q, k, ss.at[u], z_r.at[k, u], where)
+        return block(u, qd, 3 - k, ss.at[u], z_r.at[k, u], where)
 
     def z_up(u, k):
-        return z_block(u, k, lambda i: zu_s.at[i // 2, u], dev(s, z + 1, c))
+        return z_block(u, k, zu_s, dev(s, z + 1, c))
 
     def z_down(u, k):
-        return z_block(u, k, lambda i: zd_s.at[i // 2, u], dev(s, z - 1, c))
-
-    def z_in(u, k):
-        return z_block(u, k, lambda i: zu_s.at[i // 2, u], here)
+        return z_block(u, k, zd_s, dev(s, z - 1, c))
 
     def sent(u, k, up_way):
         return k < 3 or extra_to(u, up_way) == 2
@@ -153,28 +172,16 @@
         return (u + c) % 2 == 0
 
     def x_copy(u, k):
-        return block(u, q, k, lambda i: x_s.at[i // 2], lambda i: x_r.at[i, u], dev(sx, z, c))
+        return block(u, q, k, xy_s.at[0], x_r.at[k, u], dev(sx, z, c))
 
     def y_copy(u, k):
-        return block(u, q, k, lambda i: y_s.at[i // 2], lambda i: y_r.at[i, u], dev(sy, z, c))
-
-    def x_in(u, k):
-        return block(u, qx, k, lambda i: x_s.at[i // 2], lambda i: x_r.at[i, u], here)
-
-    def y_in(u, k):
-        return block(u, qy, k, lambda i: y_s.at[i // 2], lambda i: y_r.at[i, u], here)
-
-    def relay(u, of, where):
-        return block(u, of, 0, lambda i: d_s.at[i // 2, u], lambda i: d_r.at[i // 2, u], where)
+        return block(u, q, k, xy_s.at[1], y_r.at[k, u], dev(sy, z, c))
 
     def dy_copy(u):
-        return relay(u, qx, dev(sy, z, c))
+        return block(u, qx, 0, d_s.at[u], d_r.at[u], dev(sy, z, c))
 
     def dx_copy(u):
-        return relay(u, qy, dev(sx, z, c))
-
-    def d_in(u):
-        return relay(u, qd, here)
+        return block(u, qy, 0, d_s.at[u], d_r.at[u], dev(sx, z, c))
 
     for k in range(4):
         @pl.when(has_up & sent(z, k, True))
@@ -213,14 +220,47 @@
     def relayed(u):
         return (u != z) & (extra(u) == 1)
 
+    def add(u):
+        @pl.when(~relayed(u) | ~by_y(u))
+        def _():
+            got_w(x_r.at[0, u], 0)
+
+        @pl.when(~relayed(u) | by_y(u))
+        def _():
+            got_w(y_r.at[0, u], 0)
+
+        got_w(x_r.at[1, u], 1)
+        got_w(y_r.at[1, u], 1)
+
+        @pl.when(relayed(u))
+        def _():
+            got_w(d_r.at[u], 0)
+        a, b = block_dot(u)
+        acc[...] += a
+        acct[...] += b
+
     def step(d, carry):
+        for sign in (-1, 1):
+            u = z + sign * (d - 1)
+
+            @pl.when(valid(u) & (d > 1) & relayed(u))
+            def _():
+                @pl.when(by_y(u))
+                def _():
+                    got_w(x_r.at[0, u], 0)
+                    each(dy_copy(u), "start")
+
+                @pl.when(~by_y(u))
+                def _():
+                    got_w(y_r.at[0, u], 0)
+                    each(dx_copy(u), "start")
         for k in range(4):
             for sign in (-1, 1):
                 u = z + sign * d
 
                 @pl.when(valid(u) & sent(u, k, sign < 0))
                 def _():
-                    each(z_in(u, k), "wait_recv")
+                    got_w(z_r.at[k, u], k)
                     if sign < 0:
                         @pl.when(has_up)
                         def _():
@@ -232,21 +272,6 @@
                     if k < 2:
                         each(x_copy(u, k), "start")
                         each(y_copy(u, k), "start")
-            if k == 0:
-                for sign in (-1, 1):
-                    u = z + sign * (d - 1)
-
-                    @pl.when(valid(u) & (d > 1) & relayed(u))
-                    def _():
-                        @pl.when(by_y(u))
-                        def _():
-                            each(x_in(u, 0), "wait_recv")
-                            each(dy_copy(u), "start")
-
-                        @pl.when(~by_y(u))
-                        def _():
-                            each(y_in(u, 0), "wait_recv")
-                            each(dx_copy(u), "start")
             if k == 1:
                 @pl.when(d == 1)
                 def _():
@@ -261,33 +286,23 @@
 
                     @pl.when(valid(u) & (d > 2))
                     def _():
-                        @pl.when(~relayed(u) | ~by_y(u))
-                        def _():
-                            each(x_in(u, 0), "wait_recv")
-
-                        @pl.when(~relayed(u) | by_y(u))
-                        def _():
-                            each(y_in(u, 0), "wait_recv")
-
-                        each(x_in(u, 1), "wait_recv")
-                        each(y_in(u, 1), "wait_recv")
-
-                        @pl.when(relayed(u))
-                        def _():
-                            each(d_in(u), "wait_recv")
-                        a, b = block_dot(u)
-                        acc[...] += a
-                        acct[...] += b
+                        add(u)
         return carry
 
-    lax.fori_loop(1, planes + 2, step, 0)
-
-    swaps = [remote(acc.at[pl.ds(span, span)], other, acc_s.at[0], acc_r.at[0], here),
-             remote(acct.at[:, pl.ds(span, span)], othert, acc_s.at[1], acc_r.at[1], here)]
+    lax.fori_loop(1, planes + 1, step, 0)
+
+    @pl.when((z == 0) | (z == planes - 1))
+    def _():
+        add(planes - 1 - z)
+
+    give[...] = acc[span:].astype(BF16)
+    givet[...] = acct[:, span:].astype(BF16)
+    swaps = [remote(give, other, acc_s.at[0], acc_r.at[0], here),
+             remote(givet, othert, acc_s.at[1], acc_r.at[1], here)]
     each(swaps, "start")
     each(swaps, "wait")
-    latent = acc[:span] + other[...]
-    ropes = acct[:, :span] + othert[...]
+    latent = acc[:span] + other[...].astype(F32)
+    ropes = acct[:, :span] + othert[...].astype(F32)
     scaled = latent * lax.rsqrt(jnp.mean(latent * latent, axis=-1, keepdims=True) + 1e-06)
     spread[z] = (scaled * scale[...]).astype(BF16)
     swapped = jnp.concatenate([ropes[rope // 2:], ropes[:rope // 2]], axis=0)
@@ -306,47 +321,50 @@
         def _():
             getattr(turned, what)()
 
+    def got_part(sem, k):
+        @pl.when(k == 0)
+        def _():
+            got(sem, spread.at[0, pl.ds(0, part + turn_rows)])
+
+        @pl.when(k > 0)
+        def _():
+            got(sem, spread.at[0, pl.ds(0, part)])
+
     def g_copy(u, k, zi, slot, what):
-        act(k, remote(spread.at[u, cut(k)], spread.at[u, cut(k)], g_s.at[0, slot, u], g_r.at[k, u], dev(s, zi, c)),
-            remote(spreadt.at[u], spreadt.at[u], g_s.at[1, slot, u], g_r.at[PARTS, u], dev(s, zi, c)), what)
+        act(k, remote(spread.at[u, cut(k)], spread.at[u, cut(k)], g_s.at[slot, u], g_r.at[k, u], dev(s, zi, c)),
+            remote(spreadt.at[u], spreadt.at[u], g_s.at[slot, u], g_r.at[k, u], dev(s, zi, c)), what)
 
     def f_copy(u, k, where, si, what):
         act(k, remote(spread.at[u, cut(k)], xall.at[c, si, cut(k)], f_s.at[0], f_r.at[k, si], where),
-            remote(spreadt.at[u], rot_out.at[c, :, lanes(si)], f_s.at[1], f_r.at[PARTS, si], where), what)
-
-    def b_copy(u, k, what):
-        where = dev(jnp.where(k < 2, sx, sy), z, c)
-        act(k, remote(spread.at[u, cut(k)], between.at[cut(k)], f_s.at[0], m_r.at[k], where),
-            remote(spreadt.at[u], betweent, f_s.at[1], m_r.at[PARTS], where), what)
-
-    def m_copy(k, what):
-        si = jnp.where(k < 2, sx, sy)
-        where = dev(jnp.where(k < 2, sy, sx), z, c)
-        act(k, remote(between.at[cut(k)], xall.at[c, si, cut(k)], m_s.at[0], f_r.at[k, si], where),
-            remote(betweent, rot_out.at[c, :, lanes(si)], m_s.at[1], f_r.at[PARTS, si], where), what)
+            remote(spreadt.at[u], rot_out.at[c, :, lanes(si)], f_s.at[0], f_r.at[k, si], where), what)
 
     def p_own(k, what):
-        act(k, remote(spread.at[s, cut(k)], xall.at[c, s, cut(k)], p_s.at[0], p_r.at[0, s], here),
-            remote(spreadt.at[s], rot_out.at[c, :, lanes(s)], p_s.at[1], p_r.at[1, s], here), what)
+        act(k, remote(spread.at[s, cut(k)], xall.at[c, s, cut(k)], p_s.at[0], p_r.at[s], here),
+            remote(spreadt.at[s], rot_out.at[c, :, lanes(s)], p_s.at[0], p_r.at[s], here), what)
 
     def p_copy(ci, si, k, what):
         turned = rot_out.at[ci, :, lanes(si)]
-        act(k, remote(xall.at[ci, si, cut(k)], xall.at[ci, si, cut(k)], p_s.at[0], p_r.at[0, si], here),
-            remote(turned, turned, p_s.at[1], p_r.at[1, si], here), what)
+        act(k, remote(xall.at[ci, si, cut(k)], xall.at[ci, si, cut(k)], p_s.at[0], p_r.at[si], here),
+            remote(turned, turned, p_s.at[0], p_r.at[si], here), what)
+
+    def b_copy(u, k, what):
+        remotely = remote(spread.at[u, cut(k)], between.at[cut(k - PARTS // 2)], f_s.at[0], m_r.at[k - PARTS // 2], dev(sy, z, c))
+        getattr(remotely, what)()
+
+    def m_copy(k):
+        return remote(between.at[cut(k - PARTS // 2)], xall.at[c, sy, cut(k)], m_s.at[0], f_r.at[k, sy], dev(sx, z, c))
 
     def deliver(u, k):
+        round_y = (u == sd) & (k >= PARTS // 2) if near else False
+
+        @pl.when((u != s) & ~round_y if near else u != s)
+        def _():
+            f_copy(u, k, dev(u, z, c), s, "start")
+
         if near:
-            @pl.when((u != s) & (u != sd))
-            def _():
-                f_copy(u, k, dev(u, z, c), s, "start")
-
-            @pl.when(u == sd)
+            @pl.when(round_y)
             def _():
                 b_copy(u, k, "start")
-        else:
-            @pl.when(u != s)
-            def _():
-                f_copy(u, k, dev(u, z, c), s, "start")
 
         @pl.when(u == s)
         def _():
@@ -358,16 +376,7 @@
 
     def g_jump(k, what):
         act(k, remote(spread.at[z, cut(k)], spread.at[z, cut(k)], j_s.at[0], g_r.at[k, z], dev(s, end, c)),
-            remote(spreadt.at[z], spreadt.at[z], j_s.at[1], g_r.at[PARTS, z], dev(s, end, c)), what)
-
-    if jump:
-        @pl.when(across)
-        def _():
-            def far(k, carry):
-                g_jump(k, "start")
-                return carry
-
-            lax.fori_loop(0, PARTS, far, 0)
+            remote(spreadt.at[z], spreadt.at[z], j_s.at[0], g_r.at[k, z], dev(s, end, c)), what)
 
     def first(k, carry):
         @pl.when(has_up)
@@ -377,6 +386,11 @@
         @pl.when(has_down)
         def _():
             g_copy(z, k, z - 1, 1, "start")
+
+        if jump:
+            @pl.when(across)
+            def _():
+                g_jump(k, "start")
         return carry
 
     lax.fori_loop(0, PARTS, first, 0)
@@ -387,15 +401,11 @@
 
     lax.fori_loop(0, PARTS, second, 0)
 
-    def left(ref, sem):
-        remote(ref, ref, sem, sem, here).wait_send()
-
     def left_z(u, sems, up_way):
         for n in (1, 2):
             @pl.when(extra_to(u, up_way) == n)
             def _():
-                left(wlat.at[u, pl.ds(0, (2 + n) * eighth)], sems.at[0, u])
-                left(wrope.at[u, pl.ds(0, n * rpart)], sems.at[1, u])
+                left(sized((2 + n) * wide_rows + n * rpart), sems.at[u])
 
     def drain(u, carry):
         @pl.when((u >= z) & has_down)
@@ -408,13 +418,12 @@
 
         @pl.when(relayed(u))
         def _():
-            each(dy_copy(u), "wait_send")
+            left(sized(wide_rows + rpart), d_s.at[u])
         return carry
 
     lax.fori_loop(0, planes, drain, 0)
-    for sems in (x_s, y_s):
-        left(wlat.at[pl.ds(0, planes - 1), pl.ds(0, quarter)], sems.at[0])
-        left(wrope.at[pl.ds(0, planes - 1), pl.ds(0, rpart)], sems.at[1])
+    for i in range(2):
+        left(sized((planes - 1) * (2 * wide_rows + rpart)), xy_s.at[i])
 
     def fill(ci, si, x):
         keys = jnp.dot(x, up[:, :heads * kw], preferred_element_type=F32)
@@ -468,7 +477,7 @@
 
             @pl.when(valid(u) & (k >= 0) & (k < PARTS))
             def _():
-                g_copy(u, k, z, 0, "wait_recv")
+                got_part(g_r.at[k, u], k)
 
                 @pl.when(up_way & ups(u))
                 def _():
@@ -480,98 +489,85 @@
                 deliver(u, k)
 
         def arrive(k, si):
-            f_copy(0, k, here, si, "wait_recv")
+            got_part(f_r.at[k, si], k)
             p_copy(c, si, k, "start")
 
         k = n - begin(s) - LAG
-        if near:
-            @pl.when((k >= 0) & (k < PARTS))
-            def _():
+
+        @pl.when((k >= 0) & (k < PARTS))
+        def _():
+            if near:
                 arrive(k, sx)
                 arrive(k, sy)
-
-            kx = n - begin(sy) - LAG
-
-            @pl.when((kx >= 0) & (kx < 2))
-            def _():
-                m_wait(kx)
-                m_copy(kx, "start")
-
-            ky = n - begin(sx) - LAG
-
-            @pl.when((ky >= 2) & (ky < PARTS))
-            def _():
-                m_wait(ky)
-                m_copy(ky, "start")
-
-            kd = k - 3
-
-            @pl.when((kd >= 0) & (kd < PARTS))
-            def _():
-                arrive(kd, sd)
-        else:
-            @pl.when((k >= 0) & (k < PARTS))
-            def _():
+            else:
                 def other_spot(i, carry):
                     arrive(k, lax.rem(s + i, spots))
                     return carry
                 lax.fori_loop(1, spots, other_spot, 0)
 
         if near:
-            i = jnp.where(n == last - LAG, 0, jnp.where(n == last, 1, jnp.where(n > last + 2, n - last - 1, spots)))
-        else:
-            i = jnp.where(n == last - LAG, 0, jnp.where(n > last, n - last, spots))
-
-        @pl.when((i >= 0) & (i < spots))
+            ky = n - begin(sx) - LAG
+
+            @pl.when((ky >= PARTS // 2) & (ky < PARTS))
+            def _():
+                m_in = between.at[cut(ky - PARTS // 2)]
+                remote(m_in, m_in, m_s.at[0], m_r.at[ky - PARTS // 2], here).wait_recv()
+                m_copy(ky).start()
+
+            kd = k - jnp.where(k <= PARTS // 2, 1, DLAG)
+
+            @pl.when((kd >= 0) & (kd < PARTS) & ((k <= PARTS // 2) | (kd >= PARTS // 2)))
+            def _():
+                arrive(kd, sd)
+
+        i = jnp.where(n < last, n - last + LAG, n - last + 2)
+        i = jnp.where((n >= last - LAG + 2) & (n < last), -1, i)
+
+        @pl.when(i >= 0)
         def _():
             if near:
-                si = jnp.where(i == 0, s, jnp.where(i == 1, sx, jnp.where(i == 2, sy, sd)))
+                si = jnp.where(i < 2, s, jnp.where(i > 5, sd, jnp.where(lax.rem(i, 2) == 0, sx, sy)))
+                mine = (i == 0) | (i == 2) | (i == 3) | (i == 6)
             else:
-                si = lax.rem(s + i, spots)
+                si = lax.rem(s + lax.div(i, 2), spots)
+                mine = lax.rem(i, 2) == 0
 
             @pl.when(i == 0)
             def _():
                 rot_out[c, :, lanes(s)] = spreadt[s]
                 xall[c, s] = spread[s]
 
-            fill(c, si, xall[c, si])
-
-            for ref, sem in ((xall.at[1 - c, si], p_r.at[0, si]), (rot_out.at[1 - c, :, lanes(si)], p_r.at[1, si])):
-                remote(ref, ref, sem, sem, here).wait_recv()
-            fill(1 - c, si, xall[1 - c, si])
+            @pl.when(~mine)
+            def _():
+                got(p_r.at[si], spread.at[pl.ds(0, 2), pl.ds(0, middle)])
+
+            ci = jnp.where(mine, c, 1 - c)
+            fill(ci, si, xall[ci, si])
         return carry
 
-    def m_wait(k):
-        act(k, remote(between.at[cut(k)], between.at[cut(k)], m_s.at[0], m_r.at[k], here),
-            remote(betweent, betweent, m_s.at[1], m_r.at[PARTS], here), "wait_recv")
-
-    lax.fori_loop(0, last + spots + (1 if near else 0), go, 0)
+    lax.fori_loop(0, last + 2 * spots - 2, go, 0)
+
+    whole = spread.at[pl.ds(0, 2), pl.ds(0, middle)]
 
     def leave(u, carry):
         @pl.when((u <= z) & ups(u))
         def _():
-            left(spread.at[u], g_s.at[0, 0, u])
-            left(spreadt.at[u], g_s.at[1, 0, u])
+            left(whole, g_s.at[0, u])
 
         @pl.when((u >= z) & downs(u))
         def _():
-            left(spread.at[u], g_s.at[0, 1, u])
-            left(spreadt.at[u], g_s.at[1, 1, u])
+            left(whole, g_s.at[1, u])
         return carry
 
     lax.fori_loop(0, planes, leave, 0)
-    left(spread.at[pl.ds(0, planes - 1)], f_s.at[0])
-    left(spreadt.at[pl.ds(0, planes - 1)], f_s.at[1])
-    left(xall.at[0], p_s.at[0])
-    left(rot_out.at[0], p_s.at[1])
+    left(xall.at[pl.ds(0, 2), pl.ds(0, planes - 1), pl.ds(0, middle)], f_s.at[0])
+    left(xall.at[pl.ds(0, 2), pl.ds(0, spots), pl.ds(0, middle)], p_s.at[0])
     if near:
         left(between, m_s.at[0])
-        left(betweent, m_s.at[1])
     if jump:
         @pl.when(across)
         def _():
-            left(spread.at[z], j_s.at[0])
-            left(spreadt.at[z], j_s.at[1])
+            left(whole, j_s.at[0])
 
 
 def read_kernel(k_ref, v_ref, flat_ref, score_ref, rot_ref, turned_ref, plain_hbm, value_hbm, rot_hbm, read_hbm, reads, sems):
@@ -628,13 +624,14 @@
             pltpu.VMEM((planes, rope, rows), BF16),
             pltpu.VMEM((CORES * span, lat), F32),
             pltpu.VMEM((rope, CORES * span), F32),
-            pltpu.VMEM((span, lat), F32),
-            pltpu.VMEM((rope, span), F32),
+            pltpu.VMEM((span, lat), BF16),
+            pltpu.VMEM((rope, span), BF16),
+            pltpu.VMEM((span, lat), BF16),
+            pltpu.VMEM((rope, span), BF16),
             pltpu.VMEM((planes, span, lat), BF16),
             pltpu.VMEM((planes, rope, span), BF16),
             pltpu.VMEM((CORES, spots, span, lat), BF16),
-            pltpu.VMEM((span, lat), BF16),
-            pltpu.VMEM((rope, span), BF16),
+            pltpu.VMEM((span // 2, lat), BF16),
             pltpu.VMEM(key_up.shape, BF16),
             pltpu.VMEM(value_up.shape, BF16),
             pltpu.VMEM((lat, heads * (kw + vw)), BF16),
@@ -647,14 +644,14 @@
             pltpu.VMEM((1, rope), F32),
             pltpu.VMEM((1, lat), F32),
             dma((2,)), dma((3,)),
-            dma((2, planes)), dma((2, planes)), dma((6, planes)),
-            dma((2,)), dma((3, planes)), dma((2,)), dma((3, planes)),
-            dma((2, planes)), dma((2, planes)),
+            dma((planes,)), dma((planes,)), dma((4, planes)),
+            dma((2,)), dma((2, planes)), dma((2, planes)),
+            dma((planes,)), dma((planes,)),
             dma((2,)), dma((2,)),
-            dma((2, 2, planes)), dma((PARTS + 1, planes)), dma((2,)),
-            dma((2,)), dma((PARTS + 1, spots)),
-            dma((2,)), dma((PARTS + 1,)),
-            dma((2,)), dma((2, spots)),
+            dma((2, planes)), dma((PARTS, planes)), dma((1,)),
+            dma((1,)), dma((PARTS, spots)),
+            dma((1,)), dma((PARTS // 2,)),
+            dma((1,)), dma((spots,)),
             dma((8,)),
         ],
         compiler_params=pltpu.CompilerParams(collective_id=0, has_side_effects=True, vmem_limit_bytes=VMEM_BYTES),

time: 45.6 us -> 44.4 us (0.974)
  the two profiles are of different devices: /device:TPU:17 before, /device:TPU:5 now
where the time goes in v3:
time: 44.4 us; the launch traced here: 44.2 us
  Pallas kernels  43.6 us (98%)
  between operations  0.64 us (1%)
    pallas_call x1, Pallas kernels, body(): pl.pallas_call(functools.partial(move_kernel, planes, spots), out_shape=(...  42.2 us
    pallas_call x1, Pallas kernels, body(): pl.pallas_call(read_kernel, out_shape=(jax.ShapeDtypeStruct((CORES, lengt...  1.4 us

profile of v3, /device:TPU:5, one launch (start us, length us, event | category | flops | bytes accessed | tf_op | source)
XLA Modules:
  0.0 44.2 jit_solution(17910978832154719142)
XLA Ops:
  0.6 42.2 %shard_map.138 = (bf16[2,2048,128]{2,1,0:T(8,128)(2,1)S(1)}, bf16[2,2048,128]{2,1,0:T(8,128)(2,1)S(1)}, bf16[2,512,512]{2,1,0:T(8,128)(2,1)S(1)}, f32[2,4,512]{2...) custom-call(bf16[1,128,4096]{2,1,0:T(8,128)(2,1)} %tok.1, bf16[512,512]{1,0:T(8,128)(2,1)} %wl.1, ...), custom_call_target="tpu_custom_call" | custom-call | tf_op jit(solution)/shard_map/pallas_call | solution.py:611
  42.8 1.4 %shard_map.139 = (bf16[2,2048,128]{2,1,0:T(8,128)(2,1)}, bf16[2,2048,128]{2,1,0:T(8,128)(2,1)}, bf16[2,64,512]{2,1,0:T(8,128)(2,1)}, bf16[2,4,128]{2,1,0:T(4,128)(2,1)}) custom-call(bf16[2,2048,128]{2,1,0:T(8,128)(2,1)S(1)} %get-tuple-element.14.k_ref, bf16[2,2048,128]{2,1,0:T(8,128)(2,1)S(1)} %get-tuple-element.15.v_ref, ...), custom_call_target="tpu_custom_call" | custom-call | tf_op jit(solution)/shard_map/pallas_call | solution.py:659
